TPU v7x, 32 devices: a whole 2x2x4 slice. The times are simulated.
32 devices in a mesh: rep: 4 (over z), fs: 4 (over y, x), tp: 2 (over core).
Axes of the slice: x: 2, y: 2, z: 4, core: 2. Of those that a mesh axis runs over, the one named last changes fastest.
Arguments:
- hidden_in: bfloat16 [2048, 2048], P('rep'), may hold values from -6 to 6
- cotangent: bfloat16 [2048, 2048], P('rep'), may hold values from -3 to 3
- w_up: bfloat16 [2048, 8192], P('rep', ('fs', 'tp')), may hold values from -0.125 to 0.125
- w_down: bfloat16 [8192, 2048], P(('fs', 'tp'), 'rep'), may hold values from -0.0625 to 0.0625
Outputs:
- input_grad: bfloat16 [2048, 2048], P('rep')
- up_grad: float32 [2048, 8192], P('rep', ('fs', 'tp'))
- down_grad: float32 [8192, 2048], P(('fs', 'tp'), 'rep')
All inputs are finite; a program needn't handle non-finite values.
Results may differ from a plain program's by a relative error of at most 0.017.
Values may be sent and summed in bfloat16 or wider, within the bound.
A program may use at most 64 MiB of HBM per device.

v0:
```python
import functools

import jax
import jax.numpy as jnp
from jax import lax
from jax.experimental import pallas as pl
from jax.experimental.pallas import tpu as pltpu
from jax.sharding import PartitionSpec as P

MESH = pl.DeviceIdType.MESH
BF16, F32 = jnp.bfloat16, jnp.float32


def contract_last(left, right):
    return lax.dot_general(left, right, (((1,), (1,)), ((), ())), preferred_element_type=F32)


def contract_first(left, right):
    return lax.dot_general(left, right, (((0,), (0,)), ((), ())), preferred_element_type=F32)


def plain(hidden_in, cotangent, w_up, w_down):
    up_full = lax.all_gather(w_up, "rep", axis=0, tiled=True)
    back_grad = contract_last(cotangent, lax.all_gather(w_down, "rep", axis=1, tiled=True))
    preact = jnp.dot(hidden_in, up_full, preferred_element_type=F32)
    active = jnp.maximum(preact, 0.0)
    hidden = (active * active).astype(BF16)
    slopes = (2.0 * active * back_grad).astype(BF16)
    grad_upper = lax.psum_scatter(
        contract_first(hidden_in, slopes).astype(BF16), "rep", scatter_dimension=0, tiled=True
    ).astype(F32)
    lower_rows = lax.psum_scatter(
        contract_first(cotangent, hidden).astype(BF16), "rep", scatter_dimension=0, tiled=True
    ).astype(F32)
    partial_sum = contract_last(slopes, up_full).astype(BF16)
    input_grad = lax.psum(partial_sum, ("fs", "tp")).astype(F32).astype(BF16)
    return (input_grad, grad_upper, lower_rows.T)


SEMS = 256


def kernel(
    R, x_ref, g_ref, wu_in, wd_in,
    ig_ref, ru_ref, rd_ref,
    tx, tg, wu, wd, act, slopes, s_t, h_t, part, r0, r1, r2, r3, ug, dg,
    send_sems, recv_sems, local_sems,
):
    z, f, c = lax.axis_index("rep"), lax.axis_index("fs"), lax.axis_index("tp")
    tl, D = x_ref.shape
    dl, fl = wu_in.shape
    h = fl // R
    pr = tl // 8
    xx, yy = lax.rem(f, 2), lax.div(f, 2)
    fx, fy = yy * 2 + (1 - xx), (1 - yy) * 2 + xx
    f1 = fx * (1 - c) + fy * c
    f2 = fy * (1 - c) + fx * c
    f3 = 3 - f

    edge = jnp.minimum(z, R - 1 - z)
    far = jnp.where(z < R - 1 - z, 1, -1)

    def plane_at(slot):
        both = z + (slot // 2 + 1) * (2 * (slot % 2) - 1) * far
        return jnp.where(slot < 2 * edge, both, z + far * (slot + 1 - edge))

    near_first = [plane_at(slot) for slot in range(R - 1)]
    far_first = near_first[::-1]

    def beyond(p):
        return jnp.logical_or(jnp.logical_and(p < z, z < R - 1), jnp.logical_and(p > z, z > 0))

    def past(p):
        return jnp.where(p < z, z + 1, z - 1)

    def toward(p):
        return jnp.where(p > z, z + 1, z - 1)

    pending = []
    keys = {}

    def key_of(key, p):
        return keys.setdefault(key, len(keys)) * R + p

    def dev(zz=None, ff=None, cc=None):
        return {"rep": z if zz is None else zz, "fs": f if ff is None else ff, "tp": c if cc is None else cc}

    def send(src, dst, device, key, p, when=None):
        copy = pltpu.make_async_remote_copy(
            src_ref=src, dst_ref=dst, send_sem=send_sems.at[len(pending)],
            recv_sem=recv_sems.at[key_of(key, p)], device_id=device, device_id_type=MESH)
        pending.append((copy, when))
        if when is None:
            copy.start()
        else:
            pl.when(when)(copy.start)

    def arrived(dst, key, p):
        pltpu.make_async_remote_copy(
            src_ref=dst, dst_ref=dst, send_sem=send_sems.at[0],
            recv_sem=recv_sems.at[key_of(key, p)], device_id=dev(cc=1 - c), device_id_type=MESH).wait_recv()

    def rows(zz, ff, cc):
        return pl.ds(pl.multiple_of(zz * tl + (cc * 4 + ff) * pr, pr), pr)

    def piece_rows(ff, cc):
        return pl.ds(pl.multiple_of((cc * 4 + ff) * pr, pr), pr)

    barrier = pltpu.get_barrier_semaphore()
    near = [dev(zz=lax.rem(z + d, R)) for d in range(1, R)] + [dev(ff=fx), dev(ff=fy), dev(cc=1 - c)]
    for device in near:
        pl.semaphore_signal(barrier, inc=1, device_id=device, device_id_type=MESH)
    pl.semaphore_wait(barrier, len(near))

    tokens = (tx, tg)
    sources = (x_ref, g_ref)

    def up_cols(zz):
        return pl.ds(pl.multiple_of(zz * h, h), h)

    def d_block(zz):
        return pl.ds(pl.multiple_of(zz * dl, dl), dl)

    for a in (0, 1):
        for to, there in ((z + 1, z < R - 1), (z - 1, z > 0)):
            send(sources[a].at[piece_rows(f, c), :], tokens[a].at[rows(z, f, c), :],
                 dev(zz=to), ("tok", a, 0), z, when=there)

    own_rows = pl.ds(pl.multiple_of(z * tl, tl), tl)
    local = [
        pltpu.make_async_copy(x_ref, tx.at[own_rows, :], local_sems.at[0]),
        pltpu.make_async_copy(g_ref, tg.at[own_rows, :], local_sems.at[1]),
        pltpu.make_async_copy(wu_in.at[:, up_cols(z)], wu.at[d_block(z), :], local_sems.at[2]),
        pltpu.make_async_copy(wd_in.at[up_cols(z), :], wd.at[:, d_block(z)], local_sems.at[3]),
    ]
    for copy in local:
        copy.start()

    def send_weights(planes):
        for p in planes:
            send(wu_in.at[:, up_cols(p)], wu.at[d_block(z), :], dev(zz=p), ("wu",), z)
        for p in planes:
            send(wd_in.at[up_cols(p), :], wd.at[:, d_block(z)], dev(zz=p), ("wd",), z)

    def spread(at, tag, p):
        def first():
            mine = at(f, c)
            send(mine, mine, dev(ff=f1), tag + (1,), p)
            send(mine, mine, dev(ff=f2), tag + (2,), p)
            send(mine, mine, dev(cc=1 - c), tag + (4,), p)

        def second():
            p1, p2 = at(f1, c), at(f2, c)
            arrived(p1, tag + (1,), p)
            send(p1, p1, dev(ff=f2), tag + (3,), p)
            send(p1, p1, dev(cc=1 - c), tag + (5,), p)
            arrived(p2, tag + (2,), p)
            send(p2, p2, dev(cc=1 - c), tag + (6,), p)

        def third():
            p3 = at(f3, c)
            arrived(p3, tag + (3,), p)
            send(p3, p3, dev(cc=1 - c), tag + (7,), p)

        def last():
            for k, ff in ((4, f), (5, f2), (6, f1), (7, f3)):
                arrived(at(ff, 1 - c), tag + (k,), p)

        return first, second, third, last

    lasts = {}
    stages = []
    for a in (0, 1):
        for slot, p in enumerate(near_first):
            first, second, third, last = spread(
                lambda ff, cc, a=a, p=p: tokens[a].at[rows(p, ff, cc), :], ("tok", a), p)

            def opening(a=a, p=p, first=first):
                mine = tokens[a].at[rows(p, f, c), :]
                arrived(mine, ("tok", a, 0), p)
                send(mine, mine, dev(zz=past(p)), ("tok", a, 0), p, when=beyond(p))
                first()

            stages.append((opening, second, third))
            lasts[a, slot] = last
    step = min(tl, 256)

    def up_block(p):
        @pl.loop(0, tl // step)
        def _(i):
            at = pl.ds(pl.multiple_of(p * tl + i * step, step), step)
            active = jnp.maximum(jnp.dot(tx[at, :], wu[...], preferred_element_type=F32), 0.0)
            act[at, :] = active
            h_t[:, at] = jnp.transpose(active * active).astype(BF16)

    def up_blocks():
        for copy in local:
            copy.wait()
        for p in near_first:
            arrived(wu.at[d_block(p), :], ("wu",), p)
        up_block(z)
        for slot, p in enumerate(near_first):
            lasts[0, slot]()
            up_block(p)

    for i in range(len(stages) + 2):
        if i == len(stages) + 1:
            up_blocks()
        for back in (0, 1, 2):
            if 0 <= i - back < len(stages):
                stages[i - back][back]()
        if i == R - 1:
            send_weights(far_first[:R // 2])
        if i == len(stages) - 1:
            send_weights(far_first[R // 2:])

    for slot in range(R - 1):
        lasts[1, slot]()

    def down_part(p):
        at = d_block(p)
        dg[:, at] = jnp.dot(h_t[...], tg[:, at], preferred_element_type=F32).astype(BF16)

    for p in far_first:
        down_part(p)
        send(dg.at[:, d_block(p)], rd_ref.at[up_cols(z), :], dev(zz=p), ("rd",), z)
    down_part(z)
    rd_ref[up_cols(z), :] = dg[:, d_block(z)]

    for p in near_first:
        arrived(wd.at[:, d_block(p)], ("wd",), p)

    half = 4 * pr
    blocks = far_first + [z]

    def r0_rows(j, ff=None):
        if ff is None:
            return pl.ds(j * half, half)
        return pl.ds(pl.multiple_of(j * half + ff * pr, pr), pr)

    def added(*terms):
        total = terms[0].astype(F32)
        for term in terms[1:]:
            total = total + term.astype(F32)
        return total.astype(BF16)

    def core_sum(j):
        p = blocks[j]
        arrived(r0.at[r0_rows(j), :], ("r0", j), 0)
        for k, ff in ((1, f3), (0, f1), (None, f2), (None, f)):
            at = rows(p, ff, c)
            part[at, :] = added(part[at, :], r0[r0_rows(j, ff), :])
            if k is not None:
                send(part.at[at, :], r1.at[j, k], dev(ff=f1), ("r1", j, k), 0)

    for j, p in enumerate(blocks):
        @pl.loop(0, tl // step)
        def _(i, p=p):
            at = pl.ds(pl.multiple_of(p * tl + i * step, step), step)
            value = 2.0 * act[at, :] * contract_last(tg[at, :], wd[...])
            slopes[at, :] = value.astype(BF16)
            s_t[:, at] = jnp.transpose(value).astype(BF16)
            part[at, :] = contract_last(slopes[at, :], wu[...]).astype(BF16)

        theirs = pl.ds(pl.multiple_of(p * tl + (1 - c) * half, half), half)
        send(part.at[theirs, :], r0.at[r0_rows(j), :], dev(cc=1 - c), ("r0", j), 0)
        if j:
            core_sum(j - 1)
    core_sum(R - 1)

    def first_sum(j):
        for k, ff in ((1, f2), (0, f)):
            at = rows(blocks[j], ff, c)
            arrived(r1.at[j, k], ("r1", j, k), 0)
            part[at, :] = added(part[at, :], r1[j, k])
            if k:
                send(part.at[at, :], r2.at[j], dev(ff=f2), ("r2", j), 0)

    def second_sum(j):
        p = blocks[j]
        at = rows(p, f, c)
        arrived(r2.at[j], ("r2", j), 0)
        part[at, :] = added(part[at, :], r2[j])

    def line_sum(j):
        p = blocks[j]
        at = rows(p, f, c)
        side = jnp.where(p > z, 0, 1)

        @pl.when(beyond(p))
        def _():
            arrived(r3.at[p, side], ("r3",), p * 2 + side)
            part[at, :] = added(part[at, :], r3[p, side])

        send(part.at[at, :], r3.at[p, side], dev(zz=toward(p)), ("r3",), p * 2 + side)

    def own_sum():
        at = rows(z, f, c)
        for side, there in ((0, z > 0), (1, z < R - 1)):
            @pl.when(there)
            def _(side=side):
                arrived(r3.at[z, side], ("r3",), z * 2 + side)
                part[at, :] = added(part[at, :], r3[z, side])
        ig_ref[piece_rows(f, c), :] = part[at, :]

    def up_part(p):
        at = d_block(p)
        ug[at, :] = jnp.transpose(jnp.dot(s_t[...], tx[:, at], preferred_element_type=F32)).astype(BF16)

    chain = (first_sum, second_sum, line_sum)
    key_of(("r3",), 0)
    key_of("above", 0)
    for i in range(R + 2):
        for back in (2, 1, 0):
            j = i - back
            if 0 <= j < R and not (back == 2 and j == R - 1):
                chain[back](j)
        if i < R - 1:
            p = far_first[i]
            up_part(p)
            send(ug.at[d_block(p), :], ru_ref.at[:, up_cols(z)], dev(zz=p), ("ru",), z)
        if i == R - 1:
            up_part(z)
            ru_ref[:, up_cols(z)] = ug[d_block(z), :]

    own_sum()
    def part_of(n):
        rows_of = lambda ff, cc: pl.ds(pl.multiple_of((cc * 4 + ff) * pr + n * (pr // 2), pr // 2), pr // 2)
        return spread(lambda ff, cc: ig_ref.at[rows_of(ff, cc), :], ("ig", n), 0)

    for pair in zip(part_of(0), part_of(1)):
        for stage in pair:
            stage()

    for p in near_first:
        arrived(rd_ref.at[up_cols(p), :], ("rd",), p)
        arrived(ru_ref.at[:, up_cols(p)], ("ru",), p)
    for copy, when in pending:
        if when is None:
            copy.wait_send()
        else:
            pl.when(when)(copy.wait_send)
    assert len(pending) <= SEMS and len(keys) * R <= SEMS


def in_planes(R, hidden_in, cotangent, w_up, w_down):
    tl, D = hidden_in.shape
    dl, fl = w_up.shape
    T, h, pr = tl * R, fl // R, tl // 8
    vmem = pl.BlockSpec(memory_space=pltpu.VMEM)
    input_grad, up, down = pl.pallas_call(
        functools.partial(kernel, R),
        out_shape=(
            jax.ShapeDtypeStruct((tl, D), BF16),
            jax.ShapeDtypeStruct((dl, fl), BF16),
            jax.ShapeDtypeStruct((fl, dl), BF16),
        ),
        in_specs=[pl.BlockSpec(memory_space=pl.ANY)] * 4,
        out_specs=(vmem, vmem, vmem),
        scratch_shapes=[
            pltpu.VMEM((T, D), BF16),
            pltpu.VMEM((T, D), BF16),
            pltpu.VMEM((D, h), BF16),
            pltpu.VMEM((h, D), BF16),
            pltpu.VMEM((T, h), F32),
            pltpu.VMEM((T, h), BF16),
            pltpu.VMEM((h, T), BF16),
            pltpu.VMEM((h, T), BF16),
            pltpu.VMEM((T, D), BF16),
            pltpu.VMEM((R * 4 * pr, D), BF16),
            pltpu.VMEM((R, 2, pr, D), BF16),
            pltpu.VMEM((R, pr, D), BF16),
            pltpu.VMEM((R, 2, pr, D), BF16),
            pltpu.VMEM((D, h), BF16),
            pltpu.VMEM((h, D), BF16),
            pltpu.SemaphoreType.DMA((SEMS,)),
            pltpu.SemaphoreType.DMA((SEMS,)),
            pltpu.SemaphoreType.DMA((4,)),
        ],
        compiler_params=pltpu.CompilerParams(
            collective_id=0, has_side_effects=True, vmem_limit_bytes=65000 * 1024
        ),
    )(hidden_in, cotangent, w_up, w_down)
    return input_grad, up.astype(F32), down.astype(F32)


def solution(mesh):
    R, F, C = (mesh.shape[name] for name in ("rep", "fs", "tp"))
    body = functools.partial(in_planes, R) if (F, C) == (4, 2) else plain
    return jax.shard_map(
        body,
        mesh=mesh,
        in_specs=(P("rep", None), P("rep", None), P("rep", ("fs", "tp")), P(("fs", "tp"), "rep")),
        out_specs=(P("rep", None), P("rep", ("fs", "tp")), P(("fs", "tp"), "rep")),
        check_vma=False,
    )
```

profile of v0, /device:TPU:1, one launch (start us, length us, event | category | flops | bytes accessed | tf_op | source)
XLA Modules:
  0.0 170.8 jit_solution(10026405444148155733)
XLA Ops:
  0.6 163.6 %shard_map.67 = (bf16[512,2048]{1,0:T(8,128)(2,1)}, bf16[512,1024]{1,0:T(8,128)(2,1)}, bf16[1024,512]{1,0:T(8,128)(2,1)}) custom-call(bf16[512,2048]{1,0:T(8,128)(2,1)} %x_ref.1, bf16[512,2048]{1,0:T(8,128)(2,1)} %g_ref.1, bf16[512,1024]{1,0:T(8,128)(2,1)} %wu_in.1, bf16[1024,512]{1,0:T(8,128)(2,1)} %wd_in.1), custom_call_target="tpu_custom_call" | custom-call | tf_op jit(solution)/shard_map/pallas_call | solution.py:351
  164.3 0.0 copy-start.1
  164.3 2.9 %convert_element_type.6 = f32[512,1024]{1,0:T(8,128)} convert(bf16[512,1024]{1,0:T(8,128)(2,1)} %get-tuple-element.7) | non-fusion elementwise | flops 524288 | bytes 3145728 | tf_op jit(solution)/shard_map/convert_element_type | solution.py:384
  167.2 0.0 copy-done.1
  167.2 0.0 copy-start
  167.2 1.6 convert_element_type.7
  168.8 0.7 copy-done
  169.5 1.3 copy.8
Async XLA Ops:
  164.3 2.9 %copy-start.1 = (bf16[1024,512]{1,0:T(8,128)(2,1)S(1)}, bf16[1024,512]{1,0:T(8,128)(2,1)}, u32[]{:S(2)}) copy-start(bf16[1024,512]{1,0:T(8,128)(2,1)} %get-tuple-element.8) | copy-start | bytes 3145732
  167.2 2.3 %copy-start = (bf16[512,2048]{1,0:T(8,128)(2,1)S(1)}, bf16[512,2048]{1,0:T(8,128)(2,1)}, u32[]{:S(2)}) copy-start(bf16[512,2048]{1,0:T(8,128)(2,1)} %get-tuple-element.12) | copy-start | bytes 6291460
where the time goes:
time: 171 us
  Pallas kernels  164 us (96%)
  other arithmetic  4.49 us (3%)
  local copies, waits for them, and re-layouts  2.06 us (1%)
    pallas_call x1, Pallas kernels, in_planes(): pl.pallas_call(functools.partial(kernel, R), out_shape=(jax.ShapeDtypeStr...  164 us
    convert_element_type x2, other arithmetic, in_planes(): return (input_grad, up.astype(F32), down.astype(F32))  4.49 us

commit v1 on v0

v1 whole, which is shorter than its diff:
```python
import functools

import jax
import jax.numpy as jnp
from jax import lax
from jax.experimental import pallas as pl
from jax.experimental.pallas import tpu as pltpu
from jax.sharding import PartitionSpec as P

MESH = pl.DeviceIdType.MESH
BF16, F32 = jnp.bfloat16, jnp.float32


def contract_last(left, right):
    return lax.dot_general(left, right, (((1,), (1,)), ((), ())), preferred_element_type=F32)


def contract_first(left, right):
    return lax.dot_general(left, right, (((0,), (0,)), ((), ())), preferred_element_type=F32)


def plain(hidden_in, cotangent, w_up, w_down):
    up_full = lax.all_gather(w_up, "rep", axis=0, tiled=True)
    back_grad = contract_last(cotangent, lax.all_gather(w_down, "rep", axis=1, tiled=True))
    preact = jnp.dot(hidden_in, up_full, preferred_element_type=F32)
    active = jnp.maximum(preact, 0.0)
    hidden = (active * active).astype(BF16)
    slopes = (2.0 * active * back_grad).astype(BF16)
    grad_upper = lax.psum_scatter(
        contract_first(hidden_in, slopes).astype(BF16), "rep", scatter_dimension=0, tiled=True
    ).astype(F32)
    lower_rows = lax.psum_scatter(
        contract_first(cotangent, hidden).astype(BF16), "rep", scatter_dimension=0, tiled=True
    ).astype(F32)
    partial_sum = contract_last(slopes, up_full).astype(BF16)
    input_grad = lax.psum(partial_sum, ("fs", "tp")).astype(F32).astype(BF16)
    return (input_grad, grad_upper, lower_rows.T)


SC = jax.named_scope

def kernel(
    R, x_ref, g_ref, wu_in, wd_in,
    ig_ref, ru_ref, rd_ref,
    tok, wu, wd, act, slopes, s_t, h_t, part, r0, r1, r2, r3, ug, dg,
    send_sems, recv_sems, local_sems,
):
    z, f, c = lax.axis_index("rep"), lax.axis_index("fs"), lax.axis_index("tp")
    tl, D = x_ref.shape
    dl, fl = wu_in.shape
    h = fl // R
    pr = tl // 8
    half = 4 * pr
    steps = 2 * (R - 1)
    xx, yy = lax.rem(f, 2), lax.div(f, 2)
    fx, fy = yy * 2 + (1 - xx), (1 - yy) * 2 + xx
    f1 = fx * (1 - c) + fy * c
    f2 = fy * (1 - c) + fx * c
    f3 = 3 - f

    edge = jnp.minimum(z, R - 1 - z)
    far = jnp.where(z < R - 1 - z, 1, -1)
    inner = edge > 0
    outer = edge == 0

    def plane_at(slot):
        both = z + (slot // 2 + 1) * (2 * (slot % 2) - 1) * far
        return jnp.where(slot < 2 * edge, both, z + far * (slot + 1 - edge))

    near_first = [plane_at(slot) for slot in range(R - 1)]
    far_first = near_first[::-1]
    blocks = far_first + [z]

    def beyond(p):
        return jnp.logical_or(jnp.logical_and(p < z, z < R - 1), jnp.logical_and(p > z, z > 0))

    def past(p):
        return jnp.where(p < z, z + 1, z - 1)

    def toward(p):
        return jnp.where(p > z, z + 1, z - 1)

    send_names, recv_names = {}, {}

    def named(names, key, count):
        if key not in names:
            names[key] = sum(n for _, n in names.values()), count
        return names[key][0]

    def dev(zz=None, ff=None, cc=None):
        return {"rep": z if zz is None else zz, "fs": f if ff is None else ff, "tp": c if cc is None else cc}

    def remote(src, dst, device, group, key, index=0, count=1):
        return pltpu.make_async_remote_copy(
            src_ref=src, dst_ref=dst, send_sem=send_sems.at[named(send_names, group, 1)],
            recv_sem=recv_sems.at[named(recv_names, key, count) + index],
            device_id=device, device_id_type=MESH)

    def send(*args, **kw):
        remote(*args, **kw).start()

    def arrived(dst, key, index=0, count=1):
        pltpu.make_async_remote_copy(
            src_ref=dst, dst_ref=dst, send_sem=send_sems.at[0],
            recv_sem=recv_sems.at[named(recv_names, key, count) + index],
            device_id=dev(cc=1 - c), device_id_type=MESH).wait_recv()

    def sent(src, group):
        pltpu.make_async_remote_copy(
            src_ref=src, dst_ref=src, send_sem=send_sems.at[named(send_names, group, 1)],
            recv_sem=recv_sems.at[0], device_id=dev(cc=1 - c), device_id_type=MESH).wait_send()

    def rows(zz, ff, cc):
        return pl.ds(pl.multiple_of(zz * tl + (cc * 4 + ff) * pr, pr), pr)

    def core_rows(zz, cc):
        return pl.ds(pl.multiple_of(zz * tl + cc * half, half), half)

    def piece_rows(ff, cc):
        return pl.ds(pl.multiple_of((cc * 4 + ff) * pr, pr), pr)

    def up_cols(zz):
        return pl.ds(pl.multiple_of(zz * h, h), h)

    def d_block(zz):
        return pl.ds(pl.multiple_of(zz * dl, dl), dl)

    with SC("barrier"):
        barrier = pltpu.get_barrier_semaphore()
        near = [dev(zz=lax.rem(z + d, R)) for d in range(1, R)] + [dev(ff=fx), dev(ff=fy), dev(cc=1 - c)]
        for device in near:
            pl.semaphore_signal(barrier, inc=1, device_id=device, device_id_type=MESH)
        pl.semaphore_wait(barrier, len(near))

    TOK = dict(key="tok", count=2 * R)
    sources = (x_ref, g_ref)
    own_sends = []
    for a in (0, 1):
        for side, (to, there) in enumerate(((z + 1, z < R - 1), (z - 1, z > 0))):
            copy = remote(sources[a].at[piece_rows(f, c), :], tok.at[a, rows(z, f, c), :],
                          dev(zz=to), ("own", a, side), index=a * R + z, **TOK)
            pl.when(there)(copy.start)
            own_sends.append((copy, there))

    def send_up(p):
        send(wu_in.at[:, up_cols(p)], wu.at[d_block(z), :], dev(zz=p), "wu", "wu")

    def send_down(p):
        send(wd_in.at[up_cols(p), :], wd.at[:, d_block(z)], dev(zz=p), "wd", "wd")

    @pl.when(outer)
    def _():
        for p in near_first[:1] + far_first[:-1]:
            send_up(p)
        for p in far_first:
            send_down(p)

    own_rows = pl.ds(pl.multiple_of(z * tl, tl), tl)
    local = [
        pltpu.make_async_copy(x_ref, tok.at[0, own_rows, :], local_sems.at[0]),
        pltpu.make_async_copy(g_ref, tok.at[1, own_rows, :], local_sems.at[1]),
        pltpu.make_async_copy(wu_in.at[:, up_cols(z)], wu.at[d_block(z), :], local_sems.at[2]),
        pltpu.make_async_copy(wd_in.at[up_cols(z), :], wd.at[:, d_block(z)], local_sems.at[3]),
    ]
    for copy in local:
        copy.start()

    outer_order = [(a, slot) for slot in range(R - 1) for a in (0, 1)]
    inner_order = [(a, slot) for pair in range(0, R - 1, 2) for a in (0, 1)
                   for slot in range(pair, min(pair + 2, R - 1))]
    order = []
    for (ai, si), (ao, so) in zip(inner_order, outer_order):
        a = ai if ai == ao else jnp.where(inner, ai, ao)
        p = near_first[si] if si == so else jnp.where(inner, near_first[si], near_first[so])
        order.append((a, p))

    def spread(at, tag):
        group = tag + ("sent",)

        def first():
            mine = at(f, c)
            send(mine, mine, dev(ff=f1), group, tag + (1,))
            send(mine, mine, dev(ff=f2), group, tag + (2,))
            send(mine, mine, dev(cc=1 - c), group, tag + (4,))

        def second():
            p1, p2 = at(f1, c), at(f2, c)
            arrived(p1, tag + (1,))
            send(p1, p1, dev(ff=f2), group, tag + (3,))
            send(p1, p1, dev(cc=1 - c), group, tag + (4,))
            arrived(p2, tag + (2,))
            send(p2, p2, dev(cc=1 - c), group, tag + (4,))

        def third():
            p3 = at(f3, c)
            arrived(p3, tag + (3,))
            send(p3, p3, dev(cc=1 - c), group, tag + (4,))

        return first, second, third

    spreads = [
        spread(lambda ff, cc, a=a, p=p: tok.at[a, rows(p, ff, cc), :], ("tok", i))
        for i, (a, p) in enumerate(order)
    ]

    def forward(i):
        a, p = order[i]
        mine = tok.at[a, rows(p, f, c), :]
        return remote(mine, mine, dev(zz=past(p)), ("fwd", i), index=a * R + p, **TOK)

    def take(i):
        a, p = order[i]
        arrived(tok.at[a, rows(p, f, c), :], index=a * R + p, **TOK)
        pl.when(beyond(p))(forward(i).start)

    def first(i):
        with SC(f"first{i}"): spreads[i][0]()

    def second(i):
        with SC(f"second{i}"): spreads[i][1]()

    def third(i):
        with SC(f"third{i}"): spreads[i][2]()

    def last(i):
        a, p = order[i]
        with SC(f"last{i}"): arrived(tok.at[a, core_rows(p, 1 - c), :], ("tok", i, 4))

    def take_in(*which):
        @pl.when(inner)
        def _():
            for i in which:
                if i < steps:
                    with SC(f"takeI{i}"): take(i)

    def take_out(*which):
        @pl.when(outer)
        def _():
            for i in which:
                if i < steps:
                    with SC(f"takeO{i}"): take(i)

    with SC("take0"): take(0)
    first(0)
    with SC("take1"): take(1)
    first(1)
    take_in(2, 3)

    inward = [p for p in far_first]

    @pl.when(inner)
    def _():
        for p in far_first:
            pl.when((p - z) * far > 0)(functools.partial(send_up, p))

    second(0)
    take_out(2)
    first(2)
    second(1)
    third(0)
    take_in(4)
    take_out(3)
    first(3)
    second(2)
    third(1)
    take_in(5)

    @pl.when(inner)
    def _():
        for p in far_first:
            pl.when((p - z) * far < 0)(functools.partial(send_up, p))
        for p in far_first:
            send_down(p)

    second(3)
    third(2)
    take_out(4)
    first(4)
    second(4)
    third(3)
    take_out(5)
    first(5)
    second(5)
    third(4)

    step = min(tl, 256)

    def up_block(p):
        @pl.loop(0, tl // step)
        def _(i):
            at = pl.ds(pl.multiple_of(p * tl + i * step, step), step)
            active = jnp.maximum(jnp.dot(tok[0, at, :], wu[...], preferred_element_type=F32), 0.0)
            act[at, :] = active
            h_t[:, at] = jnp.transpose(active * active).astype(BF16)

    for copy in local:
        copy.wait()
    others = (R - 1) * dl
    with SC("wuwait"): arrived(wu.at[pl.ds(0, others), :], "wu")
    with SC("upz"): up_block(z)
    for i in range(4):
        last(i)
    with SC("up0"): up_block(near_first[0])
    with SC("up1"): up_block(near_first[1])
    third(5)
    last(4)
    with SC("up2"): up_block(near_first[2])
    last(5)

    def down_part(p):
        at = d_block(p)
        dg[:, at] = jnp.dot(h_t[...], tok[1, :, at], preferred_element_type=F32).astype(BF16)

    for p in far_first:
        with SC("downpart"): down_part(p)
        send(dg.at[:, d_block(p)], rd_ref.at[up_cols(z), :], dev(zz=p), "rd", "rd")
    with SC("downpartz"):
        down_part(z)
        rd_ref[up_cols(z), :] = dg[:, d_block(z)]

    with SC("wdwait"): arrived(wd.at[:, pl.ds(0, others)], "wd")

    def r0_rows(j, ff=None):
        if ff is None:
            return pl.ds(j * half, half)
        return pl.ds(pl.multiple_of(j * half + ff * pr, pr), pr)

    def added(*terms):
        total = terms[0].astype(F32)
        for term in terms[1:]:
            total = total + term.astype(F32)
        return total.astype(BF16)

    def core_sum(j):
        p = blocks[j]
        arrived(r0.at[r0_rows(j), :], ("r0", j))
        for k, ff in ((1, f3), (0, f1), (None, f2), (None, f)):
            at = rows(p, ff, c)
            part[at, :] = added(part[at, :], r0[r0_rows(j, ff), :])
            if k is not None:
                send(part.at[at, :], r1.at[j, k], dev(ff=f1), "r1", ("r1", j, k))

    def part_rows(at):
        value = 2.0 * act[at, :] * contract_last(tok[1, at, :], wd[...])
        slopes[at, :] = value.astype(BF16)
        part[at, :] = contract_last(slopes[at, :], wu[...]).astype(BF16)

    for j, p in enumerate(blocks):
        theirs = core_rows(p, 1 - c)
        with SC(f"slopesA{j}"): part_rows(theirs)
        send(part.at[theirs, :], r0.at[r0_rows(j), :], dev(cc=1 - c), "r0", ("r0", j))
        with SC(f"slopesB{j}"): part_rows(core_rows(p, c))
        if j:
            with SC(f"core{j-1}"): core_sum(j - 1)
    with SC(f"core{R-1}"): core_sum(R - 1)

    with SC("s_t"):
        @pl.loop(0, R * tl // step)
        def _(i):
            at = pl.ds(pl.multiple_of(i * step, step), step)
            s_t[:, at] = jnp.transpose(slopes[at, :].astype(F32)).astype(BF16)

    def first_sum(j):
        for k, ff in ((1, f2), (0, f)):
            at = rows(blocks[j], ff, c)
            arrived(r1.at[j, k], ("r1", j, k))
            part[at, :] = added(part[at, :], r1[j, k])
            if k:
                send(part.at[at, :], r2.at[j], dev(ff=f2), "r2", ("r2", j))

    def second_sum(j):
        at = rows(blocks[j], f, c)
        arrived(r2.at[j], ("r2", j))
        part[at, :] = added(part[at, :], r2[j])

    R3 = dict(key="r3", count=2 * R)

    def line_sum(j):
        p = blocks[j]
        at = rows(p, f, c)
        side = jnp.where(p > z, 0, 1)

        @pl.when(beyond(p))
        def _():
            arrived(r3.at[p, side], index=p * 2 + side, **R3)
            part[at, :] = added(part[at, :], r3[p, side])

        send(part.at[at, :], r3.at[p, side], dev(zz=toward(p)), "r3", index=p * 2 + side, **R3)

    def own_sum():
        at = rows(z, f, c)
        for side, there in ((0, z > 0), (1, z < R - 1)):
            @pl.when(there)
            def _(side=side):
                arrived(r3.at[z, side], index=z * 2 + side, **R3)
                part[at, :] = added(part[at, :], r3[z, side])
        ig_ref[piece_rows(f, c), :] = part[at, :]

    def up_part(p):
        at = d_block(p)
        ug[at, :] = jnp.transpose(jnp.dot(s_t[...], tok[0, :, at], preferred_element_type=F32)).astype(BF16)

    def send_up_part(p):
        with SC("uppart"): up_part(p)
        send(ug.at[d_block(p), :], ru_ref.at[:, up_cols(z)], dev(zz=p), "ru", "ru")

    chain = (first_sum, second_sum, line_sum)
    for i in range(R + 2):
        if i < R - 1:
            send_up_part(far_first[i])
        if i == R - 1:
            with SC("uppartz"):
                up_part(z)
                ru_ref[:, up_cols(z)] = ug[d_block(z), :]
        for back in (2, 1, 0):
            j = i - back
            if 0 <= j < R and not (back == 2 and j == R - 1):
                with SC(f"chain{back}.{j}"): chain[back](j)

    with SC("own"): own_sum()

    def part_of(n):
        rows_of = lambda ff, cc: pl.ds(pl.multiple_of((cc * 4 + ff) * pr + n * (pr // 2), pr // 2), pr // 2)
        return spread(lambda ff, cc: ig_ref.at[rows_of(ff, cc), :], ("ig", n))

    for k, pair in enumerate(zip(part_of(0), part_of(1))):
        for n, stage in enumerate(pair):
            with SC(f"ig{k}.{n}"): stage()
    with SC("iglast"):
        for n in (0, 1):
            arrived(ig_ref.at[pl.ds(0, half // 2), :], ("ig", n, 4))

    with SC("rdwait"): arrived(rd_ref.at[pl.ds(0, (R - 1) * h), :], "rd")
    with SC("ruwait"): arrived(ru_ref.at[:, pl.ds(0, (R - 1) * h)], "ru")

    with SC("sendwait"):
        for copy, there in own_sends:
            pl.when(there)(copy.wait_send)
        for i, (a, p) in enumerate(order):
            pl.when(beyond(p))(forward(i).wait_send)
            sent(part.at[pl.ds(0, 7 * pr), :], ("tok", i, "sent"))
        for n in (0, 1):
            sent(part.at[pl.ds(0, 7 * pr // 2), :], ("ig", n, "sent"))
        sent(wu.at[pl.ds(0, others), :], "wu")
        sent(wd.at[:, pl.ds(0, others)], "wd")
        sent(dg.at[:, pl.ds(0, others)], "rd")
        sent(ug.at[pl.ds(0, others), :], "ru")
        sent(r0, "r0")
        sent(r1, "r1")
        sent(r2, "r2")
        sent(part.at[pl.ds(0, (R - 1) * pr), :], "r3")
    for names, sems in ((send_names, send_sems), (recv_names, recv_sems)):
        assert sum(n for _, n in names.values()) == sems.shape[0], (names, sems.shape)


def in_planes(R, hidden_in, cotangent, w_up, w_down):
    tl, D = hidden_in.shape
    dl, fl = w_up.shape
    T, h, pr = tl * R, fl // R, tl // 8
    send_sems, recv_sems = 4 * R + 10, 16 * R + 4
    vmem = pl.BlockSpec(memory_space=pltpu.VMEM)
    input_grad, up, down = pl.pallas_call(
        functools.partial(kernel, R),
        out_shape=(
            pltpu.VMEM((tl, D), BF16),
            pltpu.VMEM((dl, fl), BF16),
            pltpu.VMEM((fl, dl), BF16),
        ),
        in_specs=[pl.BlockSpec(memory_space=pl.ANY)] * 4,
        out_specs=(vmem, vmem, vmem),
        scratch_shapes=[
            pltpu.VMEM((2, T, D), BF16),
            pltpu.VMEM((D, h), BF16),
            pltpu.VMEM((h, D), BF16),
            pltpu.VMEM((T, h), F32),
            pltpu.VMEM((T, h), BF16),
            pltpu.VMEM((h, T), BF16),
            pltpu.VMEM((h, T), BF16),
            pltpu.VMEM((T, D), BF16),
            pltpu.VMEM((R * 4 * pr, D), BF16),
            pltpu.VMEM((R, 2, pr, D), BF16),
            pltpu.VMEM((R, pr, D), BF16),
            pltpu.VMEM((R, 2, pr, D), BF16),
            pltpu.VMEM((D, h), BF16),
            pltpu.VMEM((h, D), BF16),
            pltpu.SemaphoreType.DMA((send_sems,)),
            pltpu.SemaphoreType.DMA((recv_sems,)),
            pltpu.SemaphoreType.DMA((4,)),
        ],
        compiler_params=pltpu.CompilerParams(
            collective_id=0, has_side_effects=True, vmem_limit_bytes=58 * 1024 * 1024
        ),
    )(hidden_in, cotangent, w_up, w_down)
    return input_grad, up.astype(F32), down.astype(F32)


def solution(mesh):
    R, F, C = (mesh.shape[name] for name in ("rep", "fs", "tp"))
    body = functools.partial(in_planes, R) if (F, C) == (4, 2) else plain
    return jax.shard_map(
        body,
        mesh=mesh,
        in_specs=(P("rep", None), P("rep", None), P("rep", ("fs", "tp")), P(("fs", "tp"), "rep")),
        out_specs=(P("rep", None), P("rep", ("fs", "tp")), P(("fs", "tp"), "rep")),
        check_vma=False,
    )
```

time: 171 us -> 160 us (0.936)
  Pallas kernels: 164 us -> 155 us
    pallas_call x1, Pallas kernels: 164 us -> 155 us  [in_planes(): pl.pallas_call(functools.partial(kernel, R), out_shape=(pltpu.VMEM((tl, D...]
where the time goes in v1:
time: 160 us
  Pallas kernels  155 us (97%)
  other arithmetic  3.18 us (2%)
    pallas_call x1, Pallas kernels, in_planes(): pl.pallas_call(functools.partial(kernel, R), out_shape=(pltpu.VMEM((tl, D...  155 us

profile of v1, /device:TPU:1, one launch (start us, length us, event | category | flops | bytes accessed | tf_op | source)
XLA Modules:
  0.0 159.8 jit_solution(1028523320489912973)
XLA Ops:
  0.6 154.6 %shard_map.67 = (bf16[512,2048]{1,0:T(8,128)(2,1)S(1)}, bf16[512,1024]{1,0:T(8,128)(2,1)S(1)}, bf16[1024,512]{1,0:T(8,128)(2,1)S(1)}) custom-call(bf16[512,2048]{1,0:T(8,128)(2,1)} %x_ref.1, bf16[512,2048]{1,0:T(8,128)(2,1)} %g_ref.1, bf16[512,1024]{1,0:T(8,128)(2,1)} %wu_in.1, bf16[1024,512]{1,0:T(8,128)(2,1)} %wd_in.1), custom_call_target="tpu_custom_call" | custom-call | tf_op jit(solution)/shard_map/pallas_call | solution.py:462
  155.3 1.3 copy.8
  156.6 1.6 convert_element_type.6
  158.2 1.6 %convert_element_type.7 = f32[1024,512]{1,0:T(8,128)} convert(bf16[1024,512]{1,0:T(8,128)(2,1)S(1)} %get-tuple-element.8) | non-fusion elementwise | flops 524288 | bytes 3145728 | tf_op jit(solution)/shard_map/convert_element_type | solution.py:494

commit v2 on v1

--- a/solution.py
+++ b/solution.py
@@ -38,6 +38,7 @@
 
 
 SC = jax.named_scope
+SUBS = 2
 
 def kernel(
     R, x_ref, g_ref, wu_in, wd_in,
@@ -51,6 +52,7 @@
     h = fl // R
     pr = tl // 8
     half = 4 * pr
+    sub = pr // SUBS
     steps = 2 * (R - 1)
     xx, yy = lax.rem(f, 2), lax.div(f, 2)
     fx, fy = yy * 2 + (1 - xx), (1 - yy) * 2 + xx
@@ -110,6 +112,9 @@
             src_ref=src, dst_ref=src, send_sem=send_sems.at[named(send_names, group, 1)],
             recv_sem=recv_sems.at[0], device_id=dev(cc=1 - c), device_id_type=MESH).wait_send()
 
+    def sub_rows(zz, ff, n):
+        return pl.ds(pl.multiple_of(zz * tl + (c * 4 + ff) * pr + n * sub, sub), sub)
+
     def rows(zz, ff, cc):
         return pl.ds(pl.multiple_of(zz * tl + (cc * 4 + ff) * pr, pr), pr)
 
@@ -134,13 +139,11 @@
 
     TOK = dict(key="tok", count=2 * R)
     sources = (x_ref, g_ref)
-    own_sends = []
-    for a in (0, 1):
-        for side, (to, there) in enumerate(((z + 1, z < R - 1), (z - 1, z > 0))):
-            copy = remote(sources[a].at[piece_rows(f, c), :], tok.at[a, rows(z, f, c), :],
-                          dev(zz=to), ("own", a, side), index=a * R + z, **TOK)
-            pl.when(there)(copy.start)
-            own_sends.append((copy, there))
+
+    def send_own(a, to):
+        copy = remote(sources[a].at[piece_rows(f, c), :], tok.at[a, rows(z, f, c), :],
+                      dev(zz=to), "own", index=a * R + z, **TOK)
+        copy.start()
 
     def send_up(p):
         send(wu_in.at[:, up_cols(p)], wu.at[d_block(z), :], dev(zz=p), "wu", "wu")
@@ -148,11 +151,23 @@
     def send_down(p):
         send(wd_in.at[up_cols(p), :], wd.at[:, d_block(z)], dev(zz=p), "wd", "wd")
 
+    for a in (0, 1):
+        send_own(a, near_first[0])
+        send_own(a, near_first[1])
+
     @pl.when(outer)
     def _():
-        for p in near_first[:1] + far_first[:-1]:
+        send_up(near_first[0])
+        send_up(near_first[1])
+        send_down(near_first[1])
+        send_down(near_first[0])
+        send_up(near_first[2])
+
+    @pl.when(inner)
+    def _():
+        for p in near_first[1:]:
             send_up(p)
-        for p in far_first:
+        for p in near_first[1:]:
             send_down(p)
 
     own_rows = pl.ds(pl.multiple_of(z * tl, tl), tl)
@@ -165,9 +180,8 @@
     for copy in local:
         copy.start()
 
-    outer_order = [(a, slot) for slot in range(R - 1) for a in (0, 1)]
-    inner_order = [(a, slot) for pair in range(0, R - 1, 2) for a in (0, 1)
-                   for slot in range(pair, min(pair + 2, R - 1))]
+    inner_order = [(0, 0), (0, 1), (0, 2), (1, 0), (1, 1), (1, 2)]
+    outer_order = [(0, 0), (1, 0), (0, 1), (0, 2), (1, 1), (1, 2)]
     order = []
     for (ai, si), (ao, so) in zip(inner_order, outer_order):
         a = ai if ai == ao else jnp.where(inner, ai, ao)
@@ -206,12 +220,12 @@
     def forward(i):
         a, p = order[i]
         mine = tok.at[a, rows(p, f, c), :]
-        return remote(mine, mine, dev(zz=past(p)), ("fwd", i), index=a * R + p, **TOK)
+        return remote(mine, mine, dev(zz=near_first[0]), "fwd", index=a * R + p, **TOK)
 
     def take(i):
         a, p = order[i]
         arrived(tok.at[a, rows(p, f, c), :], index=a * R + p, **TOK)
-        pl.when(beyond(p))(forward(i).start)
+        pl.when(jnp.logical_and(inner, p != near_first[0]))(forward(i).start)
 
     def first(i):
         with SC(f"first{i}"): spreads[i][0]()
@@ -240,46 +254,40 @@
                 if i < steps:
                     with SC(f"takeO{i}"): take(i)
 
-    with SC("take0"): take(0)
+    take_in(0)
+    take_out(0)
     first(0)
-    with SC("take1"): take(1)
+    take_in(1)
+    take_out(1)
     first(1)
-    take_in(2, 3)
-
-    inward = [p for p in far_first]
-
-    @pl.when(inner)
-    def _():
-        for p in far_first:
-            pl.when((p - z) * far > 0)(functools.partial(send_up, p))
-
+    take_in(2)
     second(0)
     take_out(2)
     first(2)
+    take_in(3, 4)
     second(1)
     third(0)
-    take_in(4)
     take_out(3)
     first(3)
+    take_in(5)
+
+
+    @pl.when(inner)
+    def _():
+        send_up(near_first[0])
+        send_down(near_first[0])
+
     second(2)
     third(1)
-    take_in(5)
-
-    @pl.when(inner)
-    def _():
-        for p in far_first:
-            pl.when((p - z) * far < 0)(functools.partial(send_up, p))
-        for p in far_first:
-            send_down(p)
-
+    take_out(4)
+    first(4)
     second(3)
     third(2)
-    take_out(4)
-    first(4)
+    take_out(5)
+    pl.when(outer)(functools.partial(send_down, near_first[2]))
+    first(5)
     second(4)
     third(3)
-    take_out(5)
-    first(5)
     second(5)
     third(4)
 
@@ -300,18 +308,17 @@
     with SC("upz"): up_block(z)
     for i in range(4):
         last(i)
-    with SC("up0"): up_block(near_first[0])
-    with SC("up1"): up_block(near_first[1])
+    for slot in range(R - 1):
+        with SC(f"up{slot}"): up_block(near_first[slot])
     third(5)
     last(4)
-    with SC("up2"): up_block(near_first[2])
     last(5)
 
     def down_part(p):
         at = d_block(p)
         dg[:, at] = jnp.dot(h_t[...], tok[1, :, at], preferred_element_type=F32).astype(BF16)
 
-    for p in far_first:
+    for p in near_first:
         with SC("downpart"): down_part(p)
         send(dg.at[:, d_block(p)], rd_ref.at[up_cols(z), :], dev(zz=p), "rd", "rd")
     with SC("downpartz"):
@@ -320,10 +327,10 @@
 
     with SC("wdwait"): arrived(wd.at[:, pl.ds(0, others)], "wd")
 
-    def r0_rows(j, ff=None):
+    def r0_rows(j, ff=None, n=0):
         if ff is None:
             return pl.ds(j * half, half)
-        return pl.ds(pl.multiple_of(j * half + ff * pr, pr), pr)
+        return pl.ds(pl.multiple_of(j * half + ff * pr + n * sub, sub), sub)
 
     def added(*terms):
         total = terms[0].astype(F32)
@@ -334,98 +341,154 @@
     def core_sum(j):
         p = blocks[j]
         arrived(r0.at[r0_rows(j), :], ("r0", j))
-        for k, ff in ((1, f3), (0, f1), (None, f2), (None, f)):
+        for n in range(SUBS):
+            for k, ff in ((1, f3), (0, f1)):
+                at = sub_rows(p, ff, n)
+                part[at, :] = added(part[at, :], r0[r0_rows(j, ff, n), :])
+                send(part.at[at, :], r1.at[j, k, n], dev(ff=f1), "r1", ("r1", j, k, n))
+        for ff in (f2, f):
             at = rows(p, ff, c)
-            part[at, :] = added(part[at, :], r0[r0_rows(j, ff), :])
-            if k is not None:
-                send(part.at[at, :], r1.at[j, k], dev(ff=f1), "r1", ("r1", j, k))
+            part[at, :] = added(part[at, :], r0[pl.ds(pl.multiple_of(j * half + ff * pr, pr), pr), :])
 
     def part_rows(at):
         value = 2.0 * act[at, :] * contract_last(tok[1, at, :], wd[...])
         slopes[at, :] = value.astype(BF16)
         part[at, :] = contract_last(slopes[at, :], wu[...]).astype(BF16)
 
+    def slopes_turned():
+        @pl.loop(0, R * tl // step)
+        def _(i):
+            at = pl.ds(pl.multiple_of(i * step, step), step)
+            s_t[:, at] = jnp.transpose(slopes[at, :].astype(F32)).astype(BF16)
+
+    def first_sum(j, n):
+        at = sub_rows(blocks[j], f2, n)
+        arrived(r1.at[j, 1, n], ("r1", j, 1, n))
+        part[at, :] = added(part[at, :], r1[j, 1, n])
+        send(part.at[at, :], r2.at[j, n], dev(ff=f2), "r2", ("r2", j, n))
+
+    def second_sum(j, n):
+        at = sub_rows(blocks[j], f, n)
+        arrived(r1.at[j, 0, n], ("r1", j, 0, n))
+        arrived(r2.at[j, n], ("r2", j, n))
+        part[at, :] = added(part[at, :], r1[j, 0, n], r2[j, n])
+
+    R3 = dict(key="r3", count=2 * R * SUBS)
+
+    def r3_at(p, side, n):
+        return (p * 2 + side) * SUBS + n
+
+    def line_sum(j, n):
+        p = blocks[j]
+        at = sub_rows(p, f, n)
+        side = jnp.where(p > z, 0, 1)
+
+        @pl.when(beyond(p))
+        def _():
+            arrived(r3.at[p, side, n], index=r3_at(p, side, n), **R3)
+            part[at, :] = added(part[at, :], r3[p, side, n])
+
+        send(part.at[at, :], r3.at[p, side, n], dev(zz=toward(p)), "r3", index=r3_at(p, side, n), **R3)
+
+    def own_sum(n):
+        at = sub_rows(z, f, n)
+        for side, there in ((0, z > 0), (1, z < R - 1)):
+            @pl.when(there)
+            def _(side=side):
+                arrived(r3.at[z, side, n], index=r3_at(z, side, n), **R3)
+                part[at, :] = added(part[at, :], r3[z, side, n])
+        ig_ref[piece_sub(f, c, n), :] = part[at, :]
+
+    def piece_sub(ff, cc, n):
+        return pl.ds(pl.multiple_of((cc * 4 + ff) * pr + n * sub, sub), sub)
+
+    def up_part(p):
+        at = d_block(p)
+        ug[at, :] = jnp.transpose(jnp.dot(s_t[...], tok[0, :, at], preferred_element_type=F32)).astype(BF16)
+
+    def send_up_part(p):
+        send(ug.at[d_block(p), :], ru_ref.at[:, up_cols(z)], dev(zz=p), "ru", "ru")
+
+    def fs(j, n):
+        with SC(f"fs{j}{n}"): first_sum(j, n)
+
+    def ss(j, n):
+        with SC(f"ss{j}{n}"): second_sum(j, n)
+        if j < R - 1:
+            @pl.when(outer)
+            def _():
+                with SC(f"lsO{j}{n}"): line_sum(j, n)
+
+    def ls(j, n):
+        @pl.when(inner)
+        def _():
+            with SC(f"lsI{j}{n}"): line_sum(j, n)
+
+    def turn(slot):
+        with SC("uppart"): up_part(far_first[slot])
+
     for j, p in enumerate(blocks):
         theirs = core_rows(p, 1 - c)
         with SC(f"slopesA{j}"): part_rows(theirs)
         send(part.at[theirs, :], r0.at[r0_rows(j), :], dev(cc=1 - c), "r0", ("r0", j))
-        with SC(f"slopesB{j}"): part_rows(core_rows(p, c))
         if j:
             with SC(f"core{j-1}"): core_sum(j - 1)
+        if j == R - 1:
+            fs(0, 0)
+        with SC(f"slopesB{j}"): part_rows(core_rows(p, c))
     with SC(f"core{R-1}"): core_sum(R - 1)
 
-    with SC("s_t"):
-        @pl.loop(0, R * tl // step)
-        def _(i):
-            at = pl.ds(pl.multiple_of(i * step, step), step)
-            s_t[:, at] = jnp.transpose(slopes[at, :].astype(F32)).astype(BF16)
-
-    def first_sum(j):
-        for k, ff in ((1, f2), (0, f)):
-            at = rows(blocks[j], ff, c)
-            arrived(r1.at[j, k], ("r1", j, k))
-            part[at, :] = added(part[at, :], r1[j, k])
-            if k:
-                send(part.at[at, :], r2.at[j], dev(ff=f2), "r2", ("r2", j))
-
-    def second_sum(j):
-        at = rows(blocks[j], f, c)
-        arrived(r2.at[j], ("r2", j))
-        part[at, :] = added(part[at, :], r2[j])
-
-    R3 = dict(key="r3", count=2 * R)
-
-    def line_sum(j):
-        p = blocks[j]
-        at = rows(p, f, c)
-        side = jnp.where(p > z, 0, 1)
-
-        @pl.when(beyond(p))
-        def _():
-            arrived(r3.at[p, side], index=p * 2 + side, **R3)
-            part[at, :] = added(part[at, :], r3[p, side])
-
-        send(part.at[at, :], r3.at[p, side], dev(zz=toward(p)), "r3", index=p * 2 + side, **R3)
-
-    def own_sum():
-        at = rows(z, f, c)
-        for side, there in ((0, z > 0), (1, z < R - 1)):
-            @pl.when(there)
-            def _(side=side):
-                arrived(r3.at[z, side], index=z * 2 + side, **R3)
-                part[at, :] = added(part[at, :], r3[z, side])
-        ig_ref[piece_rows(f, c), :] = part[at, :]
-
-    def up_part(p):
-        at = d_block(p)
-        ug[at, :] = jnp.transpose(jnp.dot(s_t[...], tok[0, :, at], preferred_element_type=F32)).astype(BF16)
-
-    def send_up_part(p):
-        with SC("uppart"): up_part(p)
-        send(ug.at[d_block(p), :], ru_ref.at[:, up_cols(z)], dev(zz=p), "ru", "ru")
-
-    chain = (first_sum, second_sum, line_sum)
-    for i in range(R + 2):
-        if i < R - 1:
-            send_up_part(far_first[i])
-        if i == R - 1:
-            with SC("uppartz"):
-                up_part(z)
-                ru_ref[:, up_cols(z)] = ug[d_block(z), :]
-        for back in (2, 1, 0):
-            j = i - back
-            if 0 <= j < R and not (back == 2 and j == R - 1):
-                with SC(f"chain{back}.{j}"): chain[back](j)
-
-    with SC("own"): own_sum()
-
-    def part_of(n):
-        rows_of = lambda ff, cc: pl.ds(pl.multiple_of((cc * 4 + ff) * pr + n * (pr // 2), pr // 2), pr // 2)
-        return spread(lambda ff, cc: ig_ref.at[rows_of(ff, cc), :], ("ig", n))
-
-    for k, pair in enumerate(zip(part_of(0), part_of(1))):
-        for n, stage in enumerate(pair):
-            with SC(f"ig{k}.{n}"): stage()
+    fs(0, 1)
+    with SC("s_t"): slopes_turned()
+    turn(0)
+    pl.when(outer)(functools.partial(send_up_part, far_first[0]))
+    ss(0, 0)
+    fs(1, 0)
+    turn(1)
+    ss(0, 1)
+    fs(1, 1)
+    turn(2)
+    pl.when(inner)(functools.partial(send_up_part, far_first[2]))
+    ss(1, 0)
+    with SC("uppartz"):
+        up_part(z)
+        ru_ref[:, up_cols(z)] = ug[d_block(z), :]
+    fs(2, 0)
+    ss(1, 1)
+    ls(0, 0)
+    fs(2, 1)
+    ss(2, 0)
+    ls(0, 1)
+    fs(3, 0)
+    ls(1, 0)
+    ss(2, 1)
+
+    @pl.when(outer)
+    def _():
+        send_up_part(far_first[1])
+        send_up_part(far_first[2])
+
+    ls(1, 1)
+
+    @pl.when(inner)
+    def _():
+        send_up_part(far_first[0])
+        send_up_part(far_first[1])
+
+    fs(3, 1)
+    ss(3, 0)
+    ls(2, 0)
+    ls(2, 1)
+
+    gather = [spread(lambda ff, cc, n=n: ig_ref.at[piece_sub(ff, cc, n), :], ("ig", n)) for n in range(SUBS)]
+    with SC("own0"): own_sum(0)
+    gather[0][0]()
+    ss(3, 1)
+    with SC("own1"): own_sum(1)
+    gather[1][0]()
+    for k in (1, 2):
+        for n in range(SUBS):
+            with SC(f"ig{k}.{n}"): gather[n][k]()
     with SC("iglast"):
         for n in (0, 1):
             arrived(ig_ref.at[pl.ds(0, half // 2), :], ("ig", n, 4))
@@ -434,10 +497,9 @@
     with SC("ruwait"): arrived(ru_ref.at[:, pl.ds(0, (R - 1) * h)], "ru")
 
     with SC("sendwait"):
-        for copy, there in own_sends:
-            pl.when(there)(copy.wait_send)
-        for i, (a, p) in enumerate(order):
-            pl.when(beyond(p))(forward(i).wait_send)
+        sent(part.at[pl.ds(0, 4 * pr), :], "own")
+        pl.when(inner)(lambda: sent(part.at[pl.ds(0, 4 * pr), :], "fwd"))
+        for i in range(steps):
             sent(part.at[pl.ds(0, 7 * pr), :], ("tok", i, "sent"))
         for n in (0, 1):
             sent(part.at[pl.ds(0, 7 * pr // 2), :], ("ig", n, "sent"))
@@ -457,7 +519,7 @@
     tl, D = hidden_in.shape
     dl, fl = w_up.shape
     T, h, pr = tl * R, fl // R, tl // 8
-    send_sems, recv_sems = 4 * R + 10, 16 * R + 4
+    send_sems, recv_sems = 2 * R + 10, 10 * R - 4 + 5 * R * SUBS + R + 4 * SUBS
     vmem = pl.BlockSpec(memory_space=pltpu.VMEM)
     input_grad, up, down = pl.pallas_call(
         functools.partial(kernel, R),
@@ -478,9 +540,9 @@
             pltpu.VMEM((h, T), BF16),
             pltpu.VMEM((T, D), BF16),
             pltpu.VMEM((R * 4 * pr, D), BF16),
-            pltpu.VMEM((R, 2, pr, D), BF16),
-            pltpu.VMEM((R, pr, D), BF16),
-            pltpu.VMEM((R, 2, pr, D), BF16),
+            pltpu.VMEM((R, 2, SUBS, pr // SUBS, D), BF16),
+            pltpu.VMEM((R, SUBS, pr // SUBS, D), BF16),
+            pltpu.VMEM((R, 2, SUBS, pr // SUBS, D), BF16),
             pltpu.VMEM((D, h), BF16),
             pltpu.VMEM((h, D), BF16),
             pltpu.SemaphoreType.DMA((send_sems,)),
@@ -496,7 +558,7 @@
 
 def solution(mesh):
     R, F, C = (mesh.shape[name] for name in ("rep", "fs", "tp"))
-    body = functools.partial(in_planes, R) if (F, C) == (4, 2) else plain
+    body = functools.partial(in_planes, R) if (R, F, C) == (4, 4, 2) else plain
     return jax.shard_map(
         body,
         mesh=mesh,

time: 160 us -> 134 us (0.84)
  Pallas kernels: 155 us -> 128 us
    pallas_call x1, Pallas kernels: 155 us -> 128 us  [in_planes(): pl.pallas_call(functools.partial(kernel, R), out_shape=(pltpu.VMEM((tl, D...]
where the time goes in v2:
time: 134 us; the launch traced here: 133 us
  Pallas kernels  128 us (96%)
  other arithmetic  3.18 us (2%)
    pallas_call x1, Pallas kernels, in_planes(): pl.pallas_call(functools.partial(kernel, R), out_shape=(pltpu.VMEM((tl, D...  128 us
    convert_element_type x2, other arithmetic, in_planes(): return (input_grad, up.astype(F32), down.astype(F32))  3.18 us

profile of v2, /device:TPU:1, one launch (start us, length us, event | category | flops | bytes accessed | tf_op | source)
XLA Modules:
  0.0 133.4 jit_solution(2789814742401534211)
XLA Ops:
  0.6 128.3 %shard_map.67 = (bf16[512,2048]{1,0:T(8,128)(2,1)S(1)}, bf16[512,1024]{1,0:T(8,128)(2,1)S(1)}, bf16[1024,512]{1,0:T(8,128)(2,1)S(1)}) custom-call(bf16[512,2048]{1,0:T(8,128)(2,1)} %x_ref.1, bf16[512,2048]{1,0:T(8,128)(2,1)} %g_ref.1, bf16[512,1024]{1,0:T(8,128)(2,1)} %wu_in.1, bf16[1024,512]{1,0:T(8,128)(2,1)} %wd_in.1), custom_call_target="tpu_custom_call" | custom-call | tf_op jit(solution)/shard_map/pallas_call | solution.py:524
  128.9 1.3 copy.8
  130.3 1.6 %convert_element_type.6 = f32[512,1024]{1,0:T(8,128)} convert(bf16[512,1024]{1,0:T(8,128)(2,1)S(1)} %get-tuple-element.7) | non-fusion elementwise | flops 524288 | bytes 3145728 | tf_op jit(solution)/shard_map/convert_element_type | solution.py:556
  131.8 1.6 %convert_element_type.7 = f32[1024,512]{1,0:T(8,128)} convert(bf16[1024,512]{1,0:T(8,128)(2,1)S(1)} %get-tuple-element.8) | non-fusion elementwise | flops 524288 | bytes 3145728 | tf_op jit(solution)/shard_map/convert_element_type | solution.py:556

commit v3 on v2

--- a/solution.py
+++ b/solution.py
@@ -38,12 +38,12 @@
 
 
 SC = jax.named_scope
-SUBS = 2
+SUBS, CHUNKS = 2, 4
 
 def kernel(
     R, x_ref, g_ref, wu_in, wd_in,
-    ig_ref, ru_ref, rd_ref,
-    tok, wu, wd, act, slopes, s_t, h_t, part, r0, r1, r2, r3, ug, dg,
+    ig_ref, ru_ref, down_ref,
+    rd_ref, stage, tok, wu, wd, act, slopes, s_t, h_t, part, r0, r1, r2, r3, ug, dg,
     send_sems, recv_sems, local_sems,
 ):
     z, f, c = lax.axis_index("rep"), lax.axis_index("fs"), lax.axis_index("tp")
@@ -130,6 +130,14 @@
     def d_block(zz):
         return pl.ds(pl.multiple_of(zz * dl, dl), dl)
 
+    sources = (x_ref, g_ref)
+    staged = [
+        pltpu.make_async_copy(sources[a].at[piece_rows(f, c), :], stage.at[a], local_sems.at[a])
+        for a in (0, 1)
+    ]
+    for copy in staged:
+        copy.start()
+
     with SC("barrier"):
         barrier = pltpu.get_barrier_semaphore()
         near = [dev(zz=lax.rem(z + d, R)) for d in range(1, R)] + [dev(ff=fx), dev(ff=fy), dev(cc=1 - c)]
@@ -138,12 +146,9 @@
         pl.semaphore_wait(barrier, len(near))
 
     TOK = dict(key="tok", count=2 * R)
-    sources = (x_ref, g_ref)
 
     def send_own(a, to):
-        copy = remote(sources[a].at[piece_rows(f, c), :], tok.at[a, rows(z, f, c), :],
-                      dev(zz=to), "own", index=a * R + z, **TOK)
-        copy.start()
+        send(stage.at[a], tok.at[a, rows(z, f, c), :], dev(zz=to), "early", index=a * R + z, **TOK)
 
     def send_up(p):
         send(wu_in.at[:, up_cols(p)], wu.at[d_block(z), :], dev(zz=p), "wu", "wu")
@@ -152,6 +157,7 @@
         send(wd_in.at[up_cols(p), :], wd.at[:, d_block(z)], dev(zz=p), "wd", "wd")
 
     for a in (0, 1):
+        staged[a].wait()
         send_own(a, near_first[0])
         send_own(a, near_first[1])
 
@@ -172,10 +178,10 @@
 
     own_rows = pl.ds(pl.multiple_of(z * tl, tl), tl)
     local = [
-        pltpu.make_async_copy(x_ref, tok.at[0, own_rows, :], local_sems.at[0]),
-        pltpu.make_async_copy(g_ref, tok.at[1, own_rows, :], local_sems.at[1]),
-        pltpu.make_async_copy(wu_in.at[:, up_cols(z)], wu.at[d_block(z), :], local_sems.at[2]),
-        pltpu.make_async_copy(wd_in.at[up_cols(z), :], wd.at[:, d_block(z)], local_sems.at[3]),
+        pltpu.make_async_copy(x_ref, tok.at[0, own_rows, :], local_sems.at[2]),
+        pltpu.make_async_copy(g_ref, tok.at[1, own_rows, :], local_sems.at[2]),
+        pltpu.make_async_copy(wu_in.at[:, up_cols(z)], wu.at[d_block(z), :], local_sems.at[3]),
+        pltpu.make_async_copy(wd_in.at[up_cols(z), :], wd.at[:, d_block(z)], local_sems.at[4]),
     ]
     for copy in local:
         copy.start()
@@ -188,8 +194,7 @@
         p = near_first[si] if si == so else jnp.where(inner, near_first[si], near_first[so])
         order.append((a, p))
 
-    def spread(at, tag):
-        group = tag + ("sent",)
+    def spread(at, tag, group):
 
         def first():
             mine = at(f, c)
@@ -213,7 +218,7 @@
         return first, second, third
 
     spreads = [
-        spread(lambda ff, cc, a=a, p=p: tok.at[a, rows(p, ff, cc), :], ("tok", i))
+        spread(lambda ff, cc, a=a, p=p: tok.at[a, rows(p, ff, cc), :], ("tok", i), "early")
         for i, (a, p) in enumerate(order)
     ]
 
@@ -301,7 +306,9 @@
             act[at, :] = active
             h_t[:, at] = jnp.transpose(active * active).astype(BF16)
 
-    for copy in local:
+    own_tokens = tok.at[:, own_rows, :]
+    pltpu.make_async_copy(own_tokens, own_tokens, local_sems.at[2]).wait()
+    for copy in local[2:]:
         copy.wait()
     others = (R - 1) * dl
     with SC("wuwait"): arrived(wu.at[pl.ds(0, others), :], "wu")
@@ -345,7 +352,7 @@
             for k, ff in ((1, f3), (0, f1)):
                 at = sub_rows(p, ff, n)
                 part[at, :] = added(part[at, :], r0[r0_rows(j, ff, n), :])
-                send(part.at[at, :], r1.at[j, k, n], dev(ff=f1), "r1", ("r1", j, k, n))
+                send(part.at[at, :], r1.at[j, k, n], dev(ff=f1), "late", ("r1", j, k, n))
         for ff in (f2, f):
             at = rows(p, ff, c)
             part[at, :] = added(part[at, :], r0[pl.ds(pl.multiple_of(j * half + ff * pr, pr), pr), :])
@@ -365,7 +372,7 @@
         at = sub_rows(blocks[j], f2, n)
         arrived(r1.at[j, 1, n], ("r1", j, 1, n))
         part[at, :] = added(part[at, :], r1[j, 1, n])
-        send(part.at[at, :], r2.at[j, n], dev(ff=f2), "r2", ("r2", j, n))
+        send(part.at[at, :], r2.at[j, n], dev(ff=f2), "late", ("r2", j, n))
 
     def second_sum(j, n):
         at = sub_rows(blocks[j], f, n)
@@ -388,7 +395,7 @@
             arrived(r3.at[p, side, n], index=r3_at(p, side, n), **R3)
             part[at, :] = added(part[at, :], r3[p, side, n])
 
-        send(part.at[at, :], r3.at[p, side, n], dev(zz=toward(p)), "r3", index=r3_at(p, side, n), **R3)
+        send(part.at[at, :], r3.at[p, side, n], dev(zz=toward(p)), "late", index=r3_at(p, side, n), **R3)
 
     def own_sum(n):
         at = sub_rows(z, f, n)
@@ -430,7 +437,7 @@
     for j, p in enumerate(blocks):
         theirs = core_rows(p, 1 - c)
         with SC(f"slopesA{j}"): part_rows(theirs)
-        send(part.at[theirs, :], r0.at[r0_rows(j), :], dev(cc=1 - c), "r0", ("r0", j))
+        send(part.at[theirs, :], r0.at[r0_rows(j), :], dev(cc=1 - c), "late", ("r0", j))
         if j:
             with SC(f"core{j-1}"): core_sum(j - 1)
         if j == R - 1:
@@ -480,7 +487,17 @@
     ls(2, 0)
     ls(2, 1)
 
-    gather = [spread(lambda ff, cc, n=n: ig_ref.at[piece_sub(ff, cc, n), :], ("ig", n)) for n in range(SUBS)]
+    with SC("earlysent"):
+        sent(tok.at[:, pl.ds(0, (7 * R - 5) * pr), :], "early")
+        pl.when(inner)(lambda: sent(part.at[pl.ds(0, 4 * pr), :], "fwd"))
+        sent(wu.at[pl.ds(0, others), :], "wu")
+        sent(wd.at[:, pl.ds(0, others)], "wd")
+        sent(dg.at[:, pl.ds(0, others)], "rd")
+    with SC("rdwait"):
+        arrived(rd_ref.at[pl.ds(0, (R - 1) * h), :], "rd")
+        down_ref[...] = rd_ref[...].astype(F32)
+
+    gather = [spread(lambda ff, cc, n=n: ig_ref.at[piece_sub(ff, cc, n), :], ("ig", n), "late") for n in range(SUBS)]
     with SC("own0"): own_sum(0)
     gather[0][0]()
     ss(3, 1)
@@ -493,24 +510,11 @@
         for n in (0, 1):
             arrived(ig_ref.at[pl.ds(0, half // 2), :], ("ig", n, 4))
 
-    with SC("rdwait"): arrived(rd_ref.at[pl.ds(0, (R - 1) * h), :], "rd")
     with SC("ruwait"): arrived(ru_ref.at[:, pl.ds(0, (R - 1) * h)], "ru")
 
     with SC("sendwait"):
-        sent(part.at[pl.ds(0, 4 * pr), :], "own")
-        pl.when(inner)(lambda: sent(part.at[pl.ds(0, 4 * pr), :], "fwd"))
-        for i in range(steps):
-            sent(part.at[pl.ds(0, 7 * pr), :], ("tok", i, "sent"))
-        for n in (0, 1):
-            sent(part.at[pl.ds(0, 7 * pr // 2), :], ("ig", n, "sent"))
-        sent(wu.at[pl.ds(0, others), :], "wu")
-        sent(wd.at[:, pl.ds(0, others)], "wd")
-        sent(dg.at[:, pl.ds(0, others)], "rd")
         sent(ug.at[pl.ds(0, others), :], "ru")
-        sent(r0, "r0")
-        sent(r1, "r1")
-        sent(r2, "r2")
-        sent(part.at[pl.ds(0, (R - 1) * pr), :], "r3")
+        sent(tok.at[:, pl.ds(0, (4 * R + 3) * pr), :], "late")
     for names, sems in ((send_names, send_sems), (recv_names, recv_sems)):
         assert sum(n for _, n in names.values()) == sems.shape[0], (names, sems.shape)
 
@@ -519,18 +523,20 @@
     tl, D = hidden_in.shape
     dl, fl = w_up.shape
     T, h, pr = tl * R, fl // R, tl // 8
-    send_sems, recv_sems = 2 * R + 10, 10 * R - 4 + 5 * R * SUBS + R + 4 * SUBS
+    send_sems, recv_sems = 7, 10 * R - 4 + 5 * R * SUBS + R + 4 * SUBS
     vmem = pl.BlockSpec(memory_space=pltpu.VMEM)
     input_grad, up, down = pl.pallas_call(
         functools.partial(kernel, R),
         out_shape=(
             pltpu.VMEM((tl, D), BF16),
             pltpu.VMEM((dl, fl), BF16),
-            pltpu.VMEM((fl, dl), BF16),
+            pltpu.VMEM((fl, dl), F32),
         ),
         in_specs=[pl.BlockSpec(memory_space=pl.ANY)] * 4,
         out_specs=(vmem, vmem, vmem),
         scratch_shapes=[
+            pltpu.VMEM((fl, dl), BF16),
+            pltpu.VMEM((2, pr, D), BF16),
             pltpu.VMEM((2, T, D), BF16),
             pltpu.VMEM((D, h), BF16),
             pltpu.VMEM((h, D), BF16),
@@ -547,13 +553,47 @@
             pltpu.VMEM((h, D), BF16),
             pltpu.SemaphoreType.DMA((send_sems,)),
             pltpu.SemaphoreType.DMA((recv_sems,)),
-            pltpu.SemaphoreType.DMA((4,)),
+            pltpu.SemaphoreType.DMA((5,)),
         ],
         compiler_params=pltpu.CompilerParams(
             collective_id=0, has_side_effects=True, vmem_limit_bytes=58 * 1024 * 1024
         ),
     )(hidden_in, cotangent, w_up, w_down)
-    return input_grad, up.astype(F32), down.astype(F32)
+    return written_out(input_grad, up, down)
+
+
+def write_out(ig_ref, up_ref, down_ref, ig_out, up_out, down_out, wide, sems):
+    copies = [
+        pltpu.make_async_copy(ig_ref, ig_out, sems.at[0]),
+        pltpu.make_async_copy(down_ref, down_out, sems.at[1]),
+    ]
+    for copy in copies:
+        copy.start()
+    n = up_ref.shape[0] // CHUNKS
+    for i in range(CHUNKS):
+        at = pl.ds(i * n, n)
+        wide[at, :] = up_ref[at, :].astype(F32)
+        copies.append(pltpu.make_async_copy(wide.at[at, :], up_out.at[at, :], sems.at[2 + i]))
+        copies[-1].start()
+    for copy in copies:
+        copy.wait()
+
+
+def written_out(input_grad, up, down):
+    vmem = pl.BlockSpec(memory_space=pltpu.VMEM)
+    there = [pltpu.with_memory_space_constraint(x, pltpu.VMEM) for x in (input_grad, up, down)]
+    return pl.pallas_call(
+        write_out,
+        out_shape=(
+            jax.ShapeDtypeStruct(input_grad.shape, BF16),
+            jax.ShapeDtypeStruct(up.shape, F32),
+            jax.ShapeDtypeStruct(down.shape, F32),
+        ),
+        in_specs=[vmem] * 3,
+        out_specs=[pl.BlockSpec(memory_space=pl.ANY)] * 3,
+        scratch_shapes=[pltpu.VMEM(up.shape, F32), pltpu.SemaphoreType.DMA((2 + CHUNKS,))],
+        compiler_params=pltpu.CompilerParams(vmem_limit_bytes=8 * 1024 * 1024),
+    )(*there)
 
 
 def solution(mesh):

time: 134 us -> 132 us (0.985)
  other arithmetic: 3.18 us -> 0 us
  Pallas kernels: 128 us -> 131 us
    convert_element_type x2 -> x0, other arithmetic: 3.18 us -> none  [in_planes(): return (input_grad, up.astype(F32), down.astype(F32))]
    pallas_call x0 -> x1, Pallas kernels: none -> 2.7 us  [written_out(): pl.pallas_call(write_out, out_shape=(jax.ShapeDtypeStruct(input_grad.shap...]
where the time goes in v3:
time: 132 us; the launch traced here: 131 us
  Pallas kernels  131 us (99%)
    pallas_call x1, Pallas kernels, in_planes(): pl.pallas_call(functools.partial(kernel, R), out_shape=(pltpu.VMEM((tl, D...  128 us
    pallas_call x1, Pallas kernels, written_out(): pl.pallas_call(write_out, out_shape=(jax.ShapeDtypeStruct(input_grad.shap...  2.7 us

profile of v3, /device:TPU:1, one launch (start us, length us, event | category | flops | bytes accessed | tf_op | source)
XLA Modules:
  0.0 131.3 jit_solution(14719499339769320017)
XLA Ops:
  0.6 127.8 %shard_map.67 = (bf16[512,2048]{1,0:T(8,128)(2,1)S(1)}, bf16[512,1024]{1,0:T(8,128)(2,1)S(1)}, f32[1024,512]{1,0:T(8,128)S(1)}) custom-call(bf16[512,2048]{1,0:T(8,128)(2,1)} %x_ref.1, bf16[512,2048]{1,0:T(8,128)(2,1)} %g_ref.1, bf16[512,1024]{1,0:T(8,128)(2,1)} %wu_in.1, bf16[1024,512]{1,0:T(8,128)(2,1)} %wd_in.1), custom_call_target="tpu_custom_call" | custom-call | tf_op jit(solution)/shard_map/pallas_call | solution.py:528
  128.5 2.7 %shard_map.68 = (bf16[512,2048]{1,0:T(8,128)(2,1)}, f32[512,1024]{1,0:T(8,128)}, f32[1024,512]{1,0:T(8,128)}) custom-call(bf16[512,2048]{1,0:T(8,128)(2,1)S(1)} %get-tuple-element.6.ig_ref, bf16[512,1024]{1,0:T(8,128)(2,1)S(1)} %get-tuple-element.7.up_ref, f32[1024,512]{1,0:T(8,128)S(1)} %get-tuple-element.8.down_ref), custom_call_target="tpu_custom_call" | custom-call | tf_op jit(solution)/shard_map/pallas_call | solution.py:585

commit v4 on v3

--- a/solution.py
+++ b/solution.py
@@ -38,7 +38,7 @@
 
 
 SC = jax.named_scope
-SUBS, CHUNKS = 2, 4
+SUBS, PIECES, CHUNKS, PARTS = 2, 4, 8, 2
 
 def kernel(
     R, x_ref, g_ref, wu_in, wd_in,
@@ -352,7 +352,8 @@
             for k, ff in ((1, f3), (0, f1)):
                 at = sub_rows(p, ff, n)
                 part[at, :] = added(part[at, :], r0[r0_rows(j, ff, n), :])
-                send(part.at[at, :], r1.at[j, k, n], dev(ff=f1), "late", ("r1", j, k, n))
+                key = ("r1", j, n) if k else ("r2", j, n)
+                send(part.at[at, :], r1.at[j, k, n], dev(ff=f1), "late", key)
         for ff in (f2, f):
             at = rows(p, ff, c)
             part[at, :] = added(part[at, :], r0[pl.ds(pl.multiple_of(j * half + ff * pr, pr), pr), :])
@@ -370,20 +371,19 @@
 
     def first_sum(j, n):
         at = sub_rows(blocks[j], f2, n)
-        arrived(r1.at[j, 1, n], ("r1", j, 1, n))
+        arrived(r1.at[j, 1, n], ("r1", j, n))
         part[at, :] = added(part[at, :], r1[j, 1, n])
         send(part.at[at, :], r2.at[j, n], dev(ff=f2), "late", ("r2", j, n))
 
     def second_sum(j, n):
         at = sub_rows(blocks[j], f, n)
-        arrived(r1.at[j, 0, n], ("r1", j, 0, n))
-        arrived(r2.at[j, n], ("r2", j, n))
+        arrived(part.at[pl.ds(0, 2 * sub), :], ("r2", j, n))
         part[at, :] = added(part[at, :], r1[j, 0, n], r2[j, n])
 
-    R3 = dict(key="r3", count=2 * R * SUBS)
-
-    def r3_at(p, side, n):
-        return (p * 2 + side) * SUBS + n
+    R3 = dict(key="r3", count=(R + 1) * SUBS)
+
+    def r3_at(p, side, n, ends):
+        return jnp.where(jnp.logical_and(side == 1, ends), R, p) * SUBS + n
 
     def line_sum(j, n):
         p = blocks[j]
@@ -392,17 +392,17 @@
 
         @pl.when(beyond(p))
         def _():
-            arrived(r3.at[p, side, n], index=r3_at(p, side, n), **R3)
+            arrived(r3.at[p, side, n], index=p * SUBS + n, **R3)
             part[at, :] = added(part[at, :], r3[p, side, n])
 
-        send(part.at[at, :], r3.at[p, side, n], dev(zz=toward(p)), "late", index=r3_at(p, side, n), **R3)
+        send(part.at[at, :], r3.at[p, side, n], dev(zz=toward(p)), "late", index=r3_at(p, side, n, p == toward(p)), **R3)
 
     def own_sum(n):
         at = sub_rows(z, f, n)
         for side, there in ((0, z > 0), (1, z < R - 1)):
             @pl.when(there)
             def _(side=side):
-                arrived(r3.at[z, side, n], index=r3_at(z, side, n), **R3)
+                arrived(r3.at[z, side, n], index=(R if side else z) * SUBS + n, **R3)
                 part[at, :] = added(part[at, :], r3[z, side, n])
         ig_ref[piece_sub(f, c, n), :] = part[at, :]
 
@@ -497,18 +497,31 @@
         arrived(rd_ref.at[pl.ds(0, (R - 1) * h), :], "rd")
         down_ref[...] = rd_ref[...].astype(F32)
 
-    gather = [spread(lambda ff, cc, n=n: ig_ref.at[piece_sub(ff, cc, n), :], ("ig", n), "late") for n in range(SUBS)]
+    size = pr // PIECES
+
+    def gathered(n):
+        def at(ff, cc):
+            return ig_ref.at[pl.ds(pl.multiple_of((cc * 4 + ff) * pr + n * size, size), size), :]
+        return spread(at, ("tok", n), "late")
+
+    gather = [gathered(n) for n in range(PIECES)]
     with SC("own0"): own_sum(0)
-    gather[0][0]()
+    for n in range(PIECES // 2):
+        gather[n][0]()
     ss(3, 1)
     with SC("own1"): own_sum(1)
-    gather[1][0]()
-    for k in (1, 2):
-        for n in range(SUBS):
-            with SC(f"ig{k}.{n}"): gather[n][k]()
+    for n in range(PIECES // 2, PIECES):
+        gather[n][0]()
+    for n in range(PIECES // 2):
+        with SC(f"ig1.{n}"): gather[n][1]()
+    for n in range(PIECES // 2):
+        with SC(f"ig1.{n+2}"): gather[n + PIECES // 2][1]()
+        with SC(f"ig2.{n}"): gather[n][2]()
+    for n in range(PIECES // 2, PIECES):
+        with SC(f"ig2.{n}"): gather[n][2]()
     with SC("iglast"):
-        for n in (0, 1):
-            arrived(ig_ref.at[pl.ds(0, half // 2), :], ("ig", n, 4))
+        for n in range(PIECES):
+            arrived(ig_ref.at[pl.ds(0, 4 * size), :], ("tok", n, 4))
 
     with SC("ruwait"): arrived(ru_ref.at[:, pl.ds(0, (R - 1) * h)], "ru")
 
@@ -523,7 +536,7 @@
     tl, D = hidden_in.shape
     dl, fl = w_up.shape
     T, h, pr = tl * R, fl // R, tl // 8
-    send_sems, recv_sems = 7, 10 * R - 4 + 5 * R * SUBS + R + 4 * SUBS
+    send_sems, recv_sems = 7, 11 * R - 4 + (3 * R + 1) * SUBS
     vmem = pl.BlockSpec(memory_space=pltpu.VMEM)
     input_grad, up, down = pl.pallas_call(
         functools.partial(kernel, R),
@@ -563,17 +576,18 @@
 
 
 def write_out(ig_ref, up_ref, down_ref, ig_out, up_out, down_out, wide, sems):
-    copies = [
-        pltpu.make_async_copy(ig_ref, ig_out, sems.at[0]),
-        pltpu.make_async_copy(down_ref, down_out, sems.at[1]),
-    ]
-    for copy in copies:
-        copy.start()
+    copies = []
+    for ref, out in ((down_ref, down_out), (ig_ref, ig_out)):
+        n = ref.shape[0] // PARTS
+        for i in range(PARTS):
+            at = pl.ds(i * n, n)
+            copies.append(pltpu.make_async_copy(ref.at[at, :], out.at[at, :], sems.at[len(copies)]))
+            copies[-1].start()
     n = up_ref.shape[0] // CHUNKS
     for i in range(CHUNKS):
         at = pl.ds(i * n, n)
         wide[at, :] = up_ref[at, :].astype(F32)
-        copies.append(pltpu.make_async_copy(wide.at[at, :], up_out.at[at, :], sems.at[2 + i]))
+        copies.append(pltpu.make_async_copy(wide.at[at, :], up_out.at[at, :], sems.at[len(copies)]))
         copies[-1].start()
     for copy in copies:
         copy.wait()
@@ -591,7 +605,7 @@
         ),
         in_specs=[vmem] * 3,
         out_specs=[pl.BlockSpec(memory_space=pl.ANY)] * 3,
-        scratch_shapes=[pltpu.VMEM(up.shape, F32), pltpu.SemaphoreType.DMA((2 + CHUNKS,))],
+        scratch_shapes=[pltpu.VMEM(up.shape, F32), pltpu.SemaphoreType.DMA((2 * PARTS + CHUNKS,))],
         compiler_params=pltpu.CompilerParams(vmem_limit_bytes=8 * 1024 * 1024),
     )(*there)
 

time: 132 us -> 132 us (level)
  no operation moved by 1% of the time
where the time goes in v4:
time: 132 us; the launch traced here: 130 us
  Pallas kernels  130 us (98%)
    pallas_call x1, Pallas kernels, in_planes(): pl.pallas_call(functools.partial(kernel, R), out_shape=(pltpu.VMEM((tl, D...  127 us
    pallas_call x1, Pallas kernels, written_out(): pl.pallas_call(write_out, out_shape=(jax.ShapeDtypeStruct(input_grad.shap...  2.74 us

profile of v4, /device:TPU:1, one launch (start us, length us, event | category | flops | bytes accessed | tf_op | source)
XLA Modules:
  0.0 130.4 jit_solution(15951235642866666524)
XLA Ops:
  0.6 126.8 %shard_map.67 = (bf16[512,2048]{1,0:T(8,128)(2,1)S(1)}, bf16[512,1024]{1,0:T(8,128)(2,1)S(1)}, f32[1024,512]{1,0:T(8,128)S(1)}) custom-call(bf16[512,2048]{1,0:T(8,128)(2,1)} %x_ref.1, bf16[512,2048]{1,0:T(8,128)(2,1)} %g_ref.1, bf16[512,1024]{1,0:T(8,128)(2,1)} %wu_in.1, bf16[1024,512]{1,0:T(8,128)(2,1)} %wd_in.1), custom_call_target="tpu_custom_call" | custom-call | tf_op jit(solution)/shard_map/pallas_call | solution.py:541
  127.5 2.7 %shard_map.68 = (bf16[512,2048]{1,0:T(8,128)(2,1)}, f32[512,1024]{1,0:T(8,128)}, f32[1024,512]{1,0:T(8,128)}) custom-call(bf16[512,2048]{1,0:T(8,128)(2,1)S(1)} %get-tuple-element.6.ig_ref, bf16[512,1024]{1,0:T(8,128)(2,1)S(1)} %get-tuple-element.7.up_ref, f32[1024,512]{1,0:T(8,128)S(1)} %get-tuple-element.8.down_ref), custom_call_target="tpu_custom_call" | custom-call | tf_op jit(solution)/shard_map/pallas_call | solution.py:599

commit v5 on v4

--- a/solution.py
+++ b/solution.py
@@ -38,7 +38,7 @@
 
 
 SC = jax.named_scope
-SUBS, PIECES, CHUNKS, PARTS = 2, 4, 8, 2
+SUBS, PIECES, CHUNKS = 2, 4, 4
 
 def kernel(
     R, x_ref, g_ref, wu_in, wd_in,
@@ -194,31 +194,31 @@
         p = near_first[si] if si == so else jnp.where(inner, near_first[si], near_first[so])
         order.append((a, p))
 
-    def spread(at, tag, group):
+    def spread(at, size, i, group):
+        tag, whole = ("tok", i), ("whole", i // 4)
 
         def first():
             mine = at(f, c)
             send(mine, mine, dev(ff=f1), group, tag + (1,))
-            send(mine, mine, dev(ff=f2), group, tag + (2,))
-            send(mine, mine, dev(cc=1 - c), group, tag + (4,))
+            send(mine, mine, dev(ff=f2), group, tag + (1,))
+            send(mine, mine, dev(cc=1 - c), group, whole)
 
         def second():
             p1, p2 = at(f1, c), at(f2, c)
-            arrived(p1, tag + (1,))
+            arrived(part.at[pl.ds(0, 2 * size), :], tag + (1,))
             send(p1, p1, dev(ff=f2), group, tag + (3,))
-            send(p1, p1, dev(cc=1 - c), group, tag + (4,))
-            arrived(p2, tag + (2,))
-            send(p2, p2, dev(cc=1 - c), group, tag + (4,))
+            send(p1, p1, dev(cc=1 - c), group, whole)
+            send(p2, p2, dev(cc=1 - c), group, whole)
 
         def third():
             p3 = at(f3, c)
             arrived(p3, tag + (3,))
-            send(p3, p3, dev(cc=1 - c), group, tag + (4,))
+            send(p3, p3, dev(cc=1 - c), group, whole)
 
         return first, second, third
 
     spreads = [
-        spread(lambda ff, cc, a=a, p=p: tok.at[a, rows(p, ff, cc), :], ("tok", i), "early")
+        spread(lambda ff, cc, a=a, p=p: tok.at[a, rows(p, ff, cc), :], pr, i, "early")
         for i, (a, p) in enumerate(order)
     ]
 
@@ -241,9 +241,9 @@
     def third(i):
         with SC(f"third{i}"): spreads[i][2]()
 
-    def last(i):
-        a, p = order[i]
-        with SC(f"last{i}"): arrived(tok.at[a, core_rows(p, 1 - c), :], ("tok", i, 4))
+    def last(k):
+        pieces = min(4, steps - 4 * k)
+        with SC(f"last{k}"): arrived(tok.at[0, pl.ds(0, pieces * half), :], ("whole", k))
 
     def take_in(*which):
         @pl.when(inner)
@@ -313,13 +313,11 @@
     others = (R - 1) * dl
     with SC("wuwait"): arrived(wu.at[pl.ds(0, others), :], "wu")
     with SC("upz"): up_block(z)
-    for i in range(4):
-        last(i)
+    last(0)
     for slot in range(R - 1):
         with SC(f"up{slot}"): up_block(near_first[slot])
     third(5)
-    last(4)
-    last(5)
+    last(1)
 
     def down_part(p):
         at = d_block(p)
@@ -502,7 +500,7 @@
     def gathered(n):
         def at(ff, cc):
             return ig_ref.at[pl.ds(pl.multiple_of((cc * 4 + ff) * pr + n * size, size), size), :]
-        return spread(at, ("tok", n), "late")
+        return spread(at, size, n, "late")
 
     gather = [gathered(n) for n in range(PIECES)]
     with SC("own0"): own_sum(0)
@@ -520,8 +518,7 @@
     for n in range(PIECES // 2, PIECES):
         with SC(f"ig2.{n}"): gather[n][2]()
     with SC("iglast"):
-        for n in range(PIECES):
-            arrived(ig_ref.at[pl.ds(0, 4 * size), :], ("tok", n, 4))
+        arrived(ig_ref.at[pl.ds(0, half), :], ("whole", 0))
 
     with SC("ruwait"): arrived(ru_ref.at[:, pl.ds(0, (R - 1) * h)], "ru")
 
@@ -536,7 +533,7 @@
     tl, D = hidden_in.shape
     dl, fl = w_up.shape
     T, h, pr = tl * R, fl // R, tl // 8
-    send_sems, recv_sems = 7, 11 * R - 4 + (3 * R + 1) * SUBS
+    send_sems, recv_sems = 7, 7 * R + 2 + (3 * R + 1) * SUBS
     vmem = pl.BlockSpec(memory_space=pltpu.VMEM)
     input_grad, up, down = pl.pallas_call(
         functools.partial(kernel, R),
@@ -576,20 +573,18 @@
 
 
 def write_out(ig_ref, up_ref, down_ref, ig_out, up_out, down_out, wide, sems):
-    copies = []
-    for ref, out in ((down_ref, down_out), (ig_ref, ig_out)):
-        n = ref.shape[0] // PARTS
-        for i in range(PARTS):
-            at = pl.ds(i * n, n)
-            copies.append(pltpu.make_async_copy(ref.at[at, :], out.at[at, :], sems.at[len(copies)]))
-            copies[-1].start()
+    whole = [
+        pltpu.make_async_copy(down_ref, down_out, sems.at[0]),
+        pltpu.make_async_copy(ig_ref, ig_out, sems.at[1]),
+    ]
+    for copy in whole:
+        copy.start()
     n = up_ref.shape[0] // CHUNKS
     for i in range(CHUNKS):
         at = pl.ds(i * n, n)
         wide[at, :] = up_ref[at, :].astype(F32)
-        copies.append(pltpu.make_async_copy(wide.at[at, :], up_out.at[at, :], sems.at[len(copies)]))
-        copies[-1].start()
-    for copy in copies:
+        pltpu.make_async_copy(wide.at[at, :], up_out.at[at, :], sems.at[2]).start()
+    for copy in whole + [pltpu.make_async_copy(wide, up_out, sems.at[2])]:
         copy.wait()
 
 
@@ -605,7 +600,7 @@
         ),
         in_specs=[vmem] * 3,
         out_specs=[pl.BlockSpec(memory_space=pl.ANY)] * 3,
-        scratch_shapes=[pltpu.VMEM(up.shape, F32), pltpu.SemaphoreType.DMA((2 * PARTS + CHUNKS,))],
+        scratch_shapes=[pltpu.VMEM(up.shape, F32), pltpu.SemaphoreType.DMA((3,))],
         compiler_params=pltpu.CompilerParams(vmem_limit_bytes=8 * 1024 * 1024),
     )(*there)
 

time: 132 us -> 132 us (level)
  no operation moved by 1% of the time
where the time goes in v5:
time: 132 us; the launch traced here: 130 us
  Pallas kernels  129 us (98%)
    pallas_call x1, Pallas kernels, in_planes(): pl.pallas_call(functools.partial(kernel, R), out_shape=(pltpu.VMEM((tl, D...  127 us
    pallas_call x1, Pallas kernels, written_out(): pl.pallas_call(write_out, out_shape=(jax.ShapeDtypeStruct(input_grad.shap...  2.67 us

profile of v5, /device:TPU:1, one launch (start us, length us, event | category | flops | bytes accessed | tf_op | source)
XLA Modules:
  0.0 130.2 jit_solution(17682646852236528198)
XLA Ops:
  0.6 126.7 %shard_map.67 = (bf16[512,2048]{1,0:T(8,128)(2,1)S(1)}, bf16[512,1024]{1,0:T(8,128)(2,1)S(1)}, f32[1024,512]{1,0:T(8,128)S(1)}) custom-call(bf16[512,2048]{1,0:T(8,128)(2,1)} %x_ref.1, bf16[512,2048]{1,0:T(8,128)(2,1)} %g_ref.1, bf16[512,1024]{1,0:T(8,128)(2,1)} %wu_in.1, bf16[1024,512]{1,0:T(8,128)(2,1)} %wd_in.1), custom_call_target="tpu_custom_call" | custom-call | tf_op jit(solution)/shard_map/pallas_call | solution.py:538
  127.4 2.7 %shard_map.68 = (bf16[512,2048]{1,0:T(8,128)(2,1)}, f32[512,1024]{1,0:T(8,128)}, f32[1024,512]{1,0:T(8,128)}) custom-call(bf16[512,2048]{1,0:T(8,128)(2,1)S(1)} %get-tuple-element.6.ig_ref, bf16[512,1024]{1,0:T(8,128)(2,1)S(1)} %get-tuple-element.7.up_ref, f32[1024,512]{1,0:T(8,128)S(1)} %get-tuple-element.8.down_ref), custom_call_target="tpu_custom_call" | custom-call | tf_op jit(solution)/shard_map/pallas_call | solution.py:594

commit v6 on v5

--- a/solution.py
+++ b/solution.py
@@ -151,10 +151,10 @@
         send(stage.at[a], tok.at[a, rows(z, f, c), :], dev(zz=to), "early", index=a * R + z, **TOK)
 
     def send_up(p):
-        send(wu_in.at[:, up_cols(p)], wu.at[d_block(z), :], dev(zz=p), "wu", "wu")
+        send(wu_in.at[:, up_cols(p)], wu.at[d_block(z), :], dev(zz=p), "early", "wu")
 
     def send_down(p):
-        send(wd_in.at[up_cols(p), :], wd.at[:, d_block(z)], dev(zz=p), "wd", "wd")
+        send(wd_in.at[up_cols(p), :], wd.at[:, d_block(z)], dev(zz=p), "early", "wd")
 
     for a in (0, 1):
         staged[a].wait()
@@ -325,7 +325,7 @@
 
     for p in near_first:
         with SC("downpart"): down_part(p)
-        send(dg.at[:, d_block(p)], rd_ref.at[up_cols(z), :], dev(zz=p), "rd", "rd")
+        send(dg.at[:, d_block(p)], rd_ref.at[up_cols(z), :], dev(zz=p), "late", "rd")
     with SC("downpartz"):
         down_part(z)
         rd_ref[up_cols(z), :] = dg[:, d_block(z)]
@@ -412,7 +412,7 @@
         ug[at, :] = jnp.transpose(jnp.dot(s_t[...], tok[0, :, at], preferred_element_type=F32)).astype(BF16)
 
     def send_up_part(p):
-        send(ug.at[d_block(p), :], ru_ref.at[:, up_cols(z)], dev(zz=p), "ru", "ru")
+        send(ug.at[d_block(p), :], ru_ref.at[:, up_cols(z)], dev(zz=p), "late", "ru")
 
     def fs(j, n):
         with SC(f"fs{j}{n}"): first_sum(j, n)
@@ -486,11 +486,8 @@
     ls(2, 1)
 
     with SC("earlysent"):
-        sent(tok.at[:, pl.ds(0, (7 * R - 5) * pr), :], "early")
+        sent(tok.at[:, pl.ds(0, (7 * R - 5) * pr + others * h // D), :], "early")
         pl.when(inner)(lambda: sent(part.at[pl.ds(0, 4 * pr), :], "fwd"))
-        sent(wu.at[pl.ds(0, others), :], "wu")
-        sent(wd.at[:, pl.ds(0, others)], "wd")
-        sent(dg.at[:, pl.ds(0, others)], "rd")
     with SC("rdwait"):
         arrived(rd_ref.at[pl.ds(0, (R - 1) * h), :], "rd")
         down_ref[...] = rd_ref[...].astype(F32)
@@ -523,8 +520,7 @@
     with SC("ruwait"): arrived(ru_ref.at[:, pl.ds(0, (R - 1) * h)], "ru")
 
     with SC("sendwait"):
-        sent(ug.at[pl.ds(0, others), :], "ru")
-        sent(tok.at[:, pl.ds(0, (4 * R + 3) * pr), :], "late")
+        sent(tok.at[:, pl.ds(0, (4 * R + 3) * pr + others * h // D), :], "late")
     for names, sems in ((send_names, send_sems), (recv_names, recv_sems)):
         assert sum(n for _, n in names.values()) == sems.shape[0], (names, sems.shape)
 
@@ -533,7 +529,7 @@
     tl, D = hidden_in.shape
     dl, fl = w_up.shape
     T, h, pr = tl * R, fl // R, tl // 8
-    send_sems, recv_sems = 7, 7 * R + 2 + (3 * R + 1) * SUBS
+    send_sems, recv_sems = 3, 7 * R + 2 + (3 * R + 1) * SUBS
     vmem = pl.BlockSpec(memory_space=pltpu.VMEM)
     input_grad, up, down = pl.pallas_call(
         functools.partial(kernel, R),

time: 132 us -> 132 us (level)
  no operation moved by 1% of the time
where the time goes in v6:
time: 132 us; the launch traced here: 130 us
  Pallas kernels  129 us (98%)
    pallas_call x1, Pallas kernels, in_planes(): pl.pallas_call(functools.partial(kernel, R), out_shape=(pltpu.VMEM((tl, D...  127 us
    pallas_call x1, Pallas kernels, written_out(): pl.pallas_call(write_out, out_shape=(jax.ShapeDtypeStruct(input_grad.shap...  2.67 us

profile of v6, /device:TPU:1, one launch (start us, length us, event | category | flops | bytes accessed | tf_op | source)
XLA Modules:
  0.0 130.2 jit_solution(221839839837230676)
XLA Ops:
  0.6 126.7 %shard_map.67 = (bf16[512,2048]{1,0:T(8,128)(2,1)S(1)}, bf16[512,1024]{1,0:T(8,128)(2,1)S(1)}, f32[1024,512]{1,0:T(8,128)S(1)}) custom-call(bf16[512,2048]{1,0:T(8,128)(2,1)} %x_ref.1, bf16[512,2048]{1,0:T(8,128)(2,1)} %g_ref.1, bf16[512,1024]{1,0:T(8,128)(2,1)} %wu_in.1, bf16[1024,512]{1,0:T(8,128)(2,1)} %wd_in.1), custom_call_target="tpu_custom_call" | custom-call | tf_op jit(solution)/shard_map/pallas_call | solution.py:534
  127.3 2.7 %shard_map.68 = (bf16[512,2048]{1,0:T(8,128)(2,1)}, f32[512,1024]{1,0:T(8,128)}, f32[1024,512]{1,0:T(8,128)}) custom-call(bf16[512,2048]{1,0:T(8,128)(2,1)S(1)} %get-tuple-element.6.ig_ref, bf16[512,1024]{1,0:T(8,128)(2,1)S(1)} %get-tuple-element.7.up_ref, f32[1024,512]{1,0:T(8,128)S(1)} %get-tuple-element.8.down_ref), custom_call_target="tpu_custom_call" | custom-call | tf_op jit(solution)/shard_map/pallas_call | solution.py:590
